TPU v7x, 32 devices: a whole 2x2x4 slice. The times are simulated.
32 devices in a mesh: sp: 8 (over z, x), tp: 4 (over y, core).
Axes of the slice: x: 2, y: 2, z: 4, core: 2. Of those that a mesh axis runs over, the one named last changes fastest.
Arguments:
- token_grid: bfloat16 [8, 2048, 512], P('sp', 'tp'), may hold values from -6 to 6
- norm_gain: bfloat16 [3, 2048], replicated, may hold values from 0.099609375 to 1.8984375
- w_query: bfloat16 [3, 2048, 2048], P(None, None, 'tp'), may hold values from -0.125 to 0.125
- w_key: bfloat16 [3, 2048, 2048], P(None, None, 'tp'), may hold values from -0.125 to 0.125
- w_value: bfloat16 [3, 2048, 2048], P(None, None, 'tp'), may hold values from -0.125 to 0.125
- w_out: bfloat16 [3, 2048, 2048], P(None, 'tp'), may hold values from -0.5 to 0.5
- rel_bias: float32 [3, 32, 8, 16], P(None, 'tp'), may hold values from -3 to 250
Outputs:
- grid_out: bfloat16 [8, 2048, 512], P('sp', 'tp')
All inputs are finite; a program needn't handle non-finite values.
Results may differ from a plain program's by a relative error of at most 0.024.
Values may be sent and summed in bfloat16 or wider, within the bound.
No kernel may reach another device: no remote copies, remote signals or barrier semaphores. Data moves between devices by JAX's collectives and lax.ppermute only.
A program may use at most 128 MiB of HBM per device.

v0:
```python
import jax
import jax.numpy as jnp
from jax import lax
from jax.sharding import PartitionSpec as P

D = 2048
HEAD_DIM = 64
WIN_R = 8
WIN_C = 16
LAYERS = 3


EPS = 1e-06


def from_behind(block, axis, distance):
    devices = range(lax.axis_size(axis))
    route = [((i - distance) % len(devices), i) for i in devices]
    return lax.ppermute(block, axis, route)


def periodic(source, columns):
    half_c = WIN_C // 2
    return jnp.concatenate(
        [source[..., columns - half_c :], source, source[..., : WIN_C - half_c - 1]], axis=-1
    )


def body(token_grid, norm_gain, w_query, w_key, w_value, w_out, rel_bias):
    current = token_grid
    heads_dev = rel_bias.shape[1]
    channels = w_query.shape[2]
    columns = token_grid.shape[2]
    half_r = WIN_R // 2
    factor = HEAD_DIM ** (-0.5)
    for layer_idx in range(LAYERS):
        gain_row = norm_gain[layer_idx].astype(jnp.float32)
        rows_query = w_query[layer_idx]
        rows_key = w_key[layer_idx]
        rows_value = w_value[layer_idx]
        raw_rows = lax.all_gather(current, "tp", axis=1, tiled=True)[0].astype(jnp.float32)
        scaled = (raw_rows * gain_row[:, None]).astype(jnp.bfloat16)
        slice_keyval = jnp.concatenate([rows_key, rows_value], axis=1)
        contract = (((0,), (0,)), ((), ()))
        acc_query = lax.dot_general(
            rows_query, scaled, contract, preferred_element_type=jnp.float32
        )
        acc_keyval = lax.dot_general(
            slice_keyval, scaled, contract, preferred_element_type=jnp.float32
        )
        squares = jnp.sum(raw_rows * raw_rows, axis=0)
        acc_query, acc_keyval, squares = (acc_query, acc_keyval, squares)
        inverse = lax.rsqrt(squares / D + EPS)
        queries = (acc_query * inverse[None, :]).astype(jnp.bfloat16)
        keyval = (acc_keyval * inverse[None, :]).astype(jnp.bfloat16)
        rows_list = []
        for slot_idx in range(WIN_R):
            distance = half_r - slot_idx
            if distance == 0:
                rows_list.append(keyval)
            else:
                rows_list.append(from_behind(keyval, "sp", distance))
        window_rows = jnp.stack(rows_list)
        key_rows = window_rows[:, :channels].reshape(WIN_R, heads_dev, HEAD_DIM, columns)
        value_rows = window_rows[:, channels:].reshape(WIN_R, heads_dev, HEAD_DIM, columns)
        query_heads = queries.reshape(heads_dev, HEAD_DIM, columns)
        bias_table = rel_bias[layer_idx]
        wide_keys = periodic(key_rows, columns)
        score_list = []
        for offset in range(WIN_C):
            shifted = wide_keys[..., offset : offset + columns]
            partial_value = jnp.einsum(
                "hdc,shdc->shc", query_heads, shifted, preferred_element_type=jnp.float32
            )
            score_list.append(
                partial_value * factor + jnp.transpose(bias_table[:, :, offset])[:, :, None]
            )
        scores = jnp.stack(score_list)
        highest = jnp.max(scores, axis=(0, 1), keepdims=True)
        weights = jnp.exp(scores - highest)
        weights = (weights / jnp.sum(weights, axis=(0, 1), keepdims=True)).astype(jnp.bfloat16)
        wide_values = periodic(value_rows, columns)
        mixed_out = jnp.zeros((heads_dev, HEAD_DIM, columns), jnp.float32)
        for offset in range(WIN_C):
            shifted = wide_values[..., offset : offset + columns]
            mixed_out = mixed_out + jnp.einsum(
                "shc,shdc->hdc", weights[offset], shifted, preferred_element_type=jnp.float32
            )
        mixed_out = mixed_out.reshape(channels, columns).astype(jnp.bfloat16)
        w_layer = w_out[layer_idx]
        update = lax.psum_scatter(
            lax.dot_general(
                w_layer, mixed_out, (((0,), (0,)), ((), ())), preferred_element_type=jnp.float32
            ).astype(jnp.bfloat16),
            "tp",
            scatter_dimension=0,
            tiled=True,
        ).astype(jnp.float32)
        current = (current[0].astype(jnp.float32) + update).astype(jnp.bfloat16)[None]
    return current


def solution(mesh):
    in_specs = (
        P("sp", "tp", None),
        P(),
        P(None, None, "tp"),
        P(None, None, "tp"),
        P(None, None, "tp"),
        P(None, "tp", None),
        P(None, "tp", None, None),
    )
    out_specs = P("sp", "tp", None)
    return jax.shard_map(body, mesh=mesh, in_specs=in_specs, out_specs=out_specs, check_vma=False)
```

profile of v0, /device:TPU:0, one launch (start us, length us, event | category | flops | bytes accessed | tf_op | source)
XLA Modules:
  0.0 1064.6 jit_solution(12954596138400243531)
XLA Ops:
  7.3 1.4 slice_convert_fusion
  8.7 8.9 slice_bitcast_fusion
  17.7 16.6 %all-gather.6.cloned.1.call-done = bf16[1,2048,512]{2,1,0:T(8,128)(2,1)} async-done(((bf16[1,512,512]{2,1,0:T(8,128)(2,1)}), bf16[1,2048,512]{2,1,0:T(8,128)(2,1)}) %all-gather.6.cloned.1.call-update) | async-done | bytes 2097168 | tf_op jit(solution)/shard_map/all_gather | solution.py:41
  34.2 2.1 fusion.159
  36.3 4.7 multiply_convert_fusion.2
  41.0 2.5 collective-permute-start
  43.5 2.4 collective-permute-start.1
  48.8 3.7 collective-permute-start.4
  52.5 3.7 bitcast_convert_fusion.2
  56.2 79.4 %collective-permute-done = bf16[1024,512]{1,0:T(8,128)(2,1)} collective-permute-done((bf16[1024,512]{1,0:T(8,128)(2,1)S(1)}, bf16[1024,512]{1,0:T(8,128)(2,1)}, u32[]{:S(2)}, u32[]{:S(2)}) %collective-permute-start) | collective-permute-done | bytes 1048608 | tf_op jit(solution)/shard_map/ppermute | solution.py:19
  135.6 1.3 bitcast_dynamic-update-slice_fusion.23
  136.9 44.4 %collective-permute-done.1 = bf16[1024,512]{1,0:T(8,128)(2,1)S(1)} collective-permute-done((bf16[1024,512]{1,0:T(8,128)(2,1)S(1)}, bf16[1024,512]{1,0:T(8,128)(2,1)S(1)}, u32[]{:S(2)}, u32[]{:S(2)}) %collective-permute-start.1) | collective-permute-done | bytes 1048608 | tf_op jit(solution)/shard_map/ppermute | solution.py:19
  182.1 43.4 %collective-permute-done.6 = bf16[1024,512]{1,0:T(8,128)(2,1)S(1)} collective-permute-done((bf16[1024,512]{1,0:T(8,128)(2,1)S(1)}, bf16[1024,512]{1,0:T(8,128)(2,1)S(1)}, u32[]{:S(2)}, u32[]{:S(2)}) %collective-permute-start.6) | collective-permute-done | bytes 1048608 | tf_op jit(solution)/shard_map/ppermute | solution.py:19
  226.7 18.0 %multiply_reduce_fusion.88 = (f32[8,512,8]{1,0,2:T(8,128)S(1)}, f32[8,512,8]{1,0,2:T(8,128)S(1)}, f32[8,512,8]{1,0,2:T(8,128)S(1)}, f32[8,512,8]{1,0,2:T(8,128)S...) fusion(bf16[8,8,64,512]{3,2,1,0:T(8,128)(2,1)S(1)} %bitcast.156, ...), kind=kLoop, calls=%fused_computation.166 | loop fusion | flops 117178368 | bytes 6356992 | tf_op jit(solution)/shard_map/hdc,shdc->shc/dot_general | solution.py:72
  245.5 20.8 %multiply_reduce_fusion.80 = (f32[8,512,8]{1,0,2:T(8,128)S(1)}, f32[8,512,8]{1,0,2:T(8,128)S(1)}, f32[8,512,8]{1,0,2:T(8,128)S(1)}, f32[8,512,8]{1,0,2:T(8,128)S...) fusion(bf16[8,8,64,7]{3,2,1,0:T(8,128)(2,1)S(1)} %slice.1007, ...), kind=kLoop, calls=%fused_computation.158 | loop fusion | flops 108789760 | bytes 10543104 | tf_op jit(solution)/shard_map/hdc,shdc->shc/dot_general | solution.py:72
  270.5 2.1 multiply_reduce_fusion.71
  272.7 9.0 multiply_reduce_fusion.73
  281.6 15.7 %multiply_reduce_fusion.78 = (f32[8,512,64]{1,2,0:T(8,128)}, f32[8,512,64]{1,2,0:T(8,128)}, f32[8,512,64]{1,2,0:T(8,128)}, f32[8,512,64]{1,2,0:T(8,128)}, f32[8,512,64]{1,2,0:T(8,128)}, /*index=5*/f32[8,512,64]{1,2,0:T(8,128)}) fusion(bf16[8,8,64,512]{3,2,1,0:T(8,128)(2,1)S(1)} %bitcast.1552, bf16[8,8,64,8]{3,2,1,0:T(8,128)(2,1)S(1)} %slice.979, ...), kind=kLoop, calls=%fused_computation.156 | loop fusion | flops 86507520 | bytes 11337728 | tf_op jit(solution)/shard_map/shc,shdc->hdc/dot_general | solution.py:86
  297.3 19.1 %multiply_reduce_fusion.70 = (f32[8,512,64]{1,2,0:T(8,128)}, f32[8,512,64]{1,2,0:T(8,128)}, f32[8,512,64]{1,2,0:T(8,128)}, f32[8,512,64]{1,2,0:T(8,128)}, f32[8,512,64]{1,2,0:T(8,128)}, /*index=5*/f32[8,512,64]{1,2,0:T(8,128)}) fusion(bf16[8,8,64,512]{3,2,1,0:T(8,128)(2,1)S(1)} %bitcast.1553, bf16[8,8,64,7]{3,2,1,0:T(8,128)(2,1)S(1)} %slice.1048, ...), kind=kLoop, calls=%fused_computation.148 | loop fusion | flops 86507520 | bytes 11329536 | tf_op jit(solution)/shard_map/shc,shdc->hdc/dot_general | solution.py:86
  316.5 6.4 add_convert_fusion.2
  322.9 4.3 fusion.193
  327.5 30.2 %reduce-scatter.4.cloned.1.call-done = bf16[512,512]{0,1:T(8,128)(2,1)} async-done(((bf16[2048,512]{0,1:T(8,128)(2,1)}), bf16[512,512]{0,1:T(8,128)(2,1)}) %reduce-scatter.4.cloned.1.call-update) | async-done | bytes 524304 | tf_op jit(solution)/shard_map/reduce_scatter | solution.py:91
  357.7 2.0 fusion.271
  359.7 22.7 %all-gather.8.cloned.1.call-done = bf16[2048,512]{0,1:T(8,128)(2,1)} async-done(((bf16[512,512]{0,1:T(8,128)(2,1)}), bf16[2048,512]{0,1:T(8,128)(2,1)}) %all-gather.8.cloned.1.call-update) | async-done | bytes 2097168 | tf_op jit(solution)/shard_map/all_gather | solution.py:41
  382.4 2.1 fusion.161
  384.5 4.6 multiply_convert_fusion.1
  389.1 2.5 collective-permute-start.7
  391.6 2.4 collective-permute-start.8
  396.3 3.7 collective-permute-start.11
  400.0 3.5 bitcast_convert_fusion.1
  403.5 80.2 %collective-permute-done.7 = bf16[1024,512]{1,0:T(8,128)(2,1)} collective-permute-done((bf16[1024,512]{1,0:T(8,128)(2,1)S(1)}, bf16[1024,512]{1,0:T(8,128)(2,1)}, u32[]{:S(2)}, u32[]{:S(2)}) %collective-permute-start.7) | collective-permute-done | bytes 1048608 | tf_op jit(solution)/shard_map/ppermute | solution.py:19
  483.7 1.3 bitcast_dynamic-update-slice_fusion.15
  485.0 44.4 %collective-permute-done.8 = bf16[1024,512]{1,0:T(8,128)(2,1)S(1)} collective-permute-done((bf16[1024,512]{1,0:T(8,128)(2,1)S(1)}, bf16[1024,512]{1,0:T(8,128)(2,1)S(1)}, u32[]{:S(2)}, u32[]{:S(2)}) %collective-permute-start.8) | collective-permute-done | bytes 1048608 | tf_op jit(solution)/shard_map/ppermute | solution.py:19
  529.9 43.6 %collective-permute-done.13 = bf16[1024,512]{1,0:T(8,128)(2,1)S(1)} collective-permute-done((bf16[1024,512]{1,0:T(8,128)(2,1)S(1)}, bf16[1024,512]{1,0:T(8,128)(2,1)S(1)}, u32[]{:S(2)}, u32[]{:S(2)}) %collective-permute-start.13) | collective-permute-done | bytes 1048608 | tf_op jit(solution)/shard_map/ppermute | solution.py:19
  575.0 18.0 %multiply_reduce_fusion.56 = (f32[8,512,8]{1,0,2:T(8,128)S(1)}, f32[8,512,8]{1,0,2:T(8,128)S(1)}, f32[8,512,8]{1,0,2:T(8,128)S(1)}, f32[8,512,8]{1,0,2:T(8,128)S...) fusion(bf16[8,8,64,512]{3,2,1,0:T(8,128)(2,1)S(1)} %bitcast.157, ...), kind=kLoop, calls=%fused_computation.134 | loop fusion | flops 117178368 | bytes 6356992 | tf_op jit(solution)/shard_map/hdc,shdc->shc/dot_general | solution.py:72
  593.8 20.8 %multiply_reduce_fusion.48 = (f32[8,512,8]{1,0,2:T(8,128)S(1)}, f32[8,512,8]{1,0,2:T(8,128)S(1)}, f32[8,512,8]{1,0,2:T(8,128)S(1)}, f32[8,512,8]{1,0,2:T(8,128)S...) fusion(bf16[8,8,64,7]{3,2,1,0:T(8,128)(2,1)S(1)} %slice.1097, ...), kind=kLoop, calls=%fused_computation.126 | loop fusion | flops 108789760 | bytes 10543104 | tf_op jit(solution)/shard_map/hdc,shdc->shc/dot_general | solution.py:72
  618.8 2.0 multiply_reduce_fusion.39
  620.9 9.1 multiply_reduce_fusion.41
  630.0 15.6 %multiply_reduce_fusion.46 = (f32[8,512,64]{1,2,0:T(8,128)}, f32[8,512,64]{1,2,0:T(8,128)}, f32[8,512,64]{1,2,0:T(8,128)}, f32[8,512,64]{1,2,0:T(8,128)}, f32[8,512,64]{1,2,0:T(8,128)}, /*index=5*/f32[8,512,64]{1,2,0:T(8,128)}) fusion(bf16[8,8,64,512]{3,2,1,0:T(8,128)(2,1)S(1)} %bitcast.1558, bf16[8,8,64,8]{3,2,1,0:T(8,128)(2,1)S(1)} %slice.1069, ...), kind=kLoop, calls=%fused_computation.124 | loop fusion | flops 86507520 | bytes 11337728 | tf_op jit(solution)/shard_map/shc,shdc->hdc/dot_general | solution.py:86
  645.6 18.8 %multiply_reduce_fusion.38 = (f32[8,512,64]{1,2,0:T(8,128)}, f32[8,512,64]{1,2,0:T(8,128)}, f32[8,512,64]{1,2,0:T(8,128)}, f32[8,512,64]{1,2,0:T(8,128)}, f32[8,512,64]{1,2,0:T(8,128)}, /*index=5*/f32[8,512,64]{1,2,0:T(8,128)}) fusion(bf16[8,8,64,512]{3,2,1,0:T(8,128)(2,1)S(1)} %bitcast.1559, bf16[8,8,64,7]{3,2,1,0:T(8,128)(2,1)S(1)} %slice.1138, ...), kind=kLoop, calls=%fused_computation.116 | loop fusion | flops 86507520 | bytes 11329536 | tf_op jit(solution)/shard_map/shc,shdc->hdc/dot_general | solution.py:86
  664.4 6.4 add_convert_fusion.1
  670.8 4.3 fusion.194
  675.2 30.4 %reduce-scatter.6.cloned.1.call-done = bf16[512,512]{0,1:T(8,128)(2,1)} async-done(((bf16[2048,512]{0,1:T(8,128)(2,1)}), bf16[512,512]{0,1:T(8,128)(2,1)}) %reduce-scatter.6.cloned.1.call-update) | async-done | bytes 524304 | tf_op jit(solution)/shard_map/reduce_scatter | solution.py:91
  705.6 2.0 add_convert_fusion.4
  707.6 22.7 %all-gather.10.cloned.1.call-done = bf16[2048,512]{0,1:T(8,128)(2,1)} async-done(((bf16[512,512]{0,1:T(8,128)(2,1)}), bf16[2048,512]{0,1:T(8,128)(2,1)}) %all-gather.10.cloned.1.call-update) | async-done | bytes 2097168 | tf_op jit(solution)/shard_map/all_gather | solution.py:41
  730.3 2.1 fusion.165
  732.4 5.6 multiply_convert_fusion
  738.0 2.4 collective-permute-start.14
  740.4 2.4 collective-permute-start.15
  745.1 3.7 collective-permute-start.18
  748.8 3.5 bitcast_convert_fusion
  752.3 80.2 %collective-permute-done.14 = bf16[1024,512]{1,0:T(8,128)(2,1)S(1)} collective-permute-done((bf16[1024,512]{1,0:T(8,128)(2,1)}, bf16[1024,512]{1,0:T(8,128)(2,1)S(1)}, u32[]{:S(2)}, u32[]{:S(2)}) %collective-permute-start.14) | collective-permute-done | bytes 1048608 | tf_op jit(solution)/shard_map/ppermute | solution.py:19
  832.6 45.8 %collective-permute-done.15 = bf16[1024,512]{1,0:T(8,128)(2,1)S(1)} collective-permute-done((bf16[1024,512]{1,0:T(8,128)(2,1)}, bf16[1024,512]{1,0:T(8,128)(2,1)S(1)}, u32[]{:S(2)}, u32[]{:S(2)}) %collective-permute-start.15) | collective-permute-done | bytes 1048608 | tf_op jit(solution)/shard_map/ppermute | solution.py:19
  878.7 1.3 bitcast_dynamic-update-slice_fusion.3
  880.1 42.4 %collective-permute-done.20 = bf16[1024,512]{1,0:T(8,128)(2,1)S(1)} collective-permute-done((bf16[1024,512]{1,0:T(8,128)(2,1)}, bf16[1024,512]{1,0:T(8,128)(2,1)S(1)}, u32[]{:S(2)}, u32[]{:S(2)}) %collective-permute-start.20) | collective-permute-done | bytes 1048608 | tf_op jit(solution)/shard_map/ppermute | solution.py:19
  924.3 18.0 %multiply_reduce_fusion.24 = (f32[8,512,8]{1,0,2:T(8,128)S(1)}, f32[8,512,8]{1,0,2:T(8,128)S(1)}, f32[8,512,8]{1,0,2:T(8,128)S(1)}, f32[8,512,8]{1,0,2:T(8,128)S...) fusion(bf16[8,8,64,512]{3,2,1,0:T(8,128)(2,1)S(1)} %bitcast.157, ...), kind=kLoop, calls=%fused_computation.102 | loop fusion | flops 117178368 | bytes 6356992 | tf_op jit(solution)/shard_map/hdc,shdc->shc/dot_general | solution.py:72
  943.0 20.8 %multiply_reduce_fusion.16 = (f32[8,512,8]{1,0,2:T(8,128)S(1)}, f32[8,512,8]{1,0,2:T(8,128)S(1)}, f32[8,512,8]{1,0,2:T(8,128)S(1)}, f32[8,512,8]{1,0,2:T(8,128)S...) fusion(bf16[8,8,64,7]{3,2,1,0:T(8,128)(2,1)S(1)} %slice.1187, ...), kind=kLoop, calls=%fused_computation.94 | loop fusion | flops 108789760 | bytes 10543104 | tf_op jit(solution)/shard_map/hdc,shdc->shc/dot_general | solution.py:72
  968.1 2.1 multiply_reduce_fusion.7
  970.1 9.0 multiply_reduce_fusion.9
  979.2 15.6 %multiply_reduce_fusion.14 = (f32[8,512,64]{1,2,0:T(8,128)}, f32[8,512,64]{1,2,0:T(8,128)}, f32[8,512,64]{1,2,0:T(8,128)}, f32[8,512,64]{1,2,0:T(8,128)}, f32[8,512,64]{1,2,0:T(8,128)}, /*index=5*/f32[8,512,64]{1,2,0:T(8,128)}) fusion(bf16[8,8,64,512]{3,2,1,0:T(8,128)(2,1)S(1)} %bitcast.1564, bf16[8,8,64,8]{3,2,1,0:T(8,128)(2,1)S(1)} %slice.1159, ...), kind=kLoop, calls=%fused_computation.92 | loop fusion | flops 86507520 | bytes 11337728 | tf_op jit(solution)/shard_map/shc,shdc->hdc/dot_general | solution.py:86
  994.8 18.8 %multiply_reduce_fusion.6 = (f32[8,512,64]{1,2,0:T(8,128)}, f32[8,512,64]{1,2,0:T(8,128)}, f32[8,512,64]{1,2,0:T(8,128)}, f32[8,512,64]{1,2,0:T(8,128)}, f32[8,512,64]{1,2,0:T(8,128)}, /*index=5*/f32[8,512,64]{1,2,0:T(8,128)}) fusion(bf16[8,8,64,512]{3,2,1,0:T(8,128)(2,1)S(1)} %bitcast.1565, bf16[8,8,64,7]{3,2,1,0:T(8,128)(2,1)S(1)} %slice.1228, ...), kind=kLoop, calls=%fused_computation.84 | loop fusion | flops 86507520 | bytes 11329536 | tf_op jit(solution)/shard_map/shc,shdc->hdc/dot_general | solution.py:86
  1013.6 6.4 add_convert_fusion
  1020.0 4.3 fusion.195
  1024.3 31.1 %reduce-scatter.8.cloned.1.call-done = bf16[512,512]{0,1:T(8,128)(2,1)} async-done(((bf16[2048,512]{0,1:T(8,128)(2,1)}), bf16[512,512]{0,1:T(8,128)(2,1)}) %reduce-scatter.8.cloned.1.call-update) | async-done | bytes 524304 | tf_op jit(solution)/shard_map/reduce_scatter | solution.py:91
  (281 shorter events, 31.7 us)
Async XLA Ops:
  6.5 27.7 %all-gather.6.cloned.1.call-start = ((), (), s32[]{:S(2)}) async-start(), calls=%async_computation.3 | async-start | bytes 2621440 | tf_op jit(solution)/shard_map/all_gather | solution.py:41
  7.3 350.4 %reduce-scatter.4.cloned.1.call-start = ((), (), s32[]{:S(2)}) async-start(), calls=%async_computation.4 | async-start | bytes 2621440 | tf_op jit(solution)/shard_map/reduce_scatter | solution.py:91
  36.3 9.5 copy-start.18
  41.0 94.6 %collective-permute-start = (bf16[1024,512]{1,0:T(8,128)(2,1)S(1)}, bf16[1024,512]{1,0:T(8,128)(2,1)}, u32[]{:S(2)}, u32[]{:S(2)}) collective-permute-start(bf16[1024,512]{1,0:T(8,128)(2,1)S(1)} %multiply_convert_fusion.2), channel_id=1, source_target_pairs={{16,0},{20,4},{24,8},{28,12},{0,16},{4,20},{8,24},{12,28},{17,1},{... | collective-permute-start | bytes 3145736 | tf_op jit(solution)/shard_map/ppermute | solution.py:19
  43.5 137.8 %collective-permute-start.1 = (bf16[1024,512]{1,0:T(8,128)(2,1)S(1)}, bf16[1024,512]{1,0:T(8,128)(2,1)S(1)}, u32[]{:S(2)}, u32[]{:S(2)}) collective-permute-start(bf16[1024,512]{1,0:T(8,128)(2,1)S(1)} %multiply_convert_fusion.2), channel_id=1, source_target_pairs={{20,0},{24,4},{28,8},{0,12},{4,16},{8,20},{12,24},{16,28},{21,1},{... | collective-permute-start | bytes 3145736 | tf_op jit(solution)/shard_map/ppermute | solution.py:19
  46.6 135.1 %collective-permute-start.2 = (bf16[1024,512]{1,0:T(8,128)(2,1)S(1)}, bf16[1024,512]{1,0:T(8,128)(2,1)S(1)}, u32[]{:S(2)}, u32[]{:S(2)}) collective-permute-start(bf16[1024,512]{1,0:T(8,128)(2,1)S(1)} %multiply_convert_fusion.2), channel_id=1, source_target_pairs={{24,0},{28,4},{0,8},{4,12},{8,16},{12,20},{16,24},{20,28},{25,1},{... | collective-permute-start | bytes 3145736 | tf_op jit(solution)/shard_map/ppermute | solution.py:19
  47.8 134.0 %collective-permute-start.3 = (bf16[1024,512]{1,0:T(8,128)(2,1)S(1)}, bf16[1024,512]{1,0:T(8,128)(2,1)S(1)}, u32[]{:S(2)}, u32[]{:S(2)}) collective-permute-start(bf16[1024,512]{1,0:T(8,128)(2,1)S(1)} %multiply_convert_fusion.2), channel_id=1, source_target_pairs={{28,0},{0,4},{4,8},{8,12},{12,16},{16,20},{20,24},{24,28},{29,1},{... | collective-permute-start | bytes 3145736 | tf_op jit(solution)/shard_map/ppermute | solution.py:19
  48.8 133.1 %collective-permute-start.4 = (bf16[1024,512]{1,0:T(8,128)(2,1)S(1)}, bf16[1024,512]{1,0:T(8,128)(2,1)S(1)}, u32[]{:S(2)}, u32[]{:S(2)}) collective-permute-start(bf16[1024,512]{1,0:T(8,128)(2,1)S(1)} %multiply_convert_fusion.2), channel_id=1, source_target_pairs={{4,0},{8,4},{12,8},{16,12},{20,16},{24,20},{28,24},{0,28},{5,1},{9... | collective-permute-start | bytes 3145736 | tf_op jit(solution)/shard_map/ppermute | solution.py:19
  135.6 46.4 %collective-permute-start.5 = (bf16[1024,512]{1,0:T(8,128)(2,1)S(1)}, bf16[1024,512]{1,0:T(8,128)(2,1)S(1)}, u32[]{:S(2)}, u32[]{:S(2)}) collective-permute-start(bf16[1024,512]{1,0:T(8,128)(2,1)S(1)} %multiply_convert_fusion.2), channel_id=1, source_target_pairs={{8,0},{12,4},{16,8},{20,12},{24,16},{28,20},{0,24},{4,28},{9,1},{1... | collective-permute-start | bytes 3145736 | tf_op jit(solution)/shard_map/ppermute | solution.py:19
  181.3 44.2 %collective-permute-start.6 = (bf16[1024,512]{1,0:T(8,128)(2,1)S(1)}, bf16[1024,512]{1,0:T(8,128)(2,1)S(1)}, u32[]{:S(2)}, u32[]{:S(2)}) collective-permute-start(bf16[1024,512]{1,0:T(8,128)(2,1)S(1)} %multiply_convert_fusion.2), channel_id=1, source_target_pairs={{12,0},{16,4},{20,8},{24,12},{28,16},{0,20},{4,24},{8,28},{13,1},{... | collective-permute-start | bytes 3145736 | tf_op jit(solution)/shard_map/ppermute | solution.py:19
  297.3 19.1 %copy-start.2 = (f32[8,512,64]{1,2,0:T(8,128)S(1)}, f32[8,512,64]{1,2,0:T(8,128)}, u32[]{:S(2)}) copy-start(f32[8,512,64]{1,2,0:T(8,128)} %get-tuple-element.84) | copy-start | bytes 3145732
  297.3 19.1 %copy-start.3 = (f32[8,512,64]{1,2,0:T(8,128)S(1)}, f32[8,512,64]{1,2,0:T(8,128)}, u32[]{:S(2)}) copy-start(f32[8,512,64]{1,2,0:T(8,128)} %get-tuple-element.85) | copy-start | bytes 3145732
  297.3 19.1 %copy-start.4 = (f32[8,512,64]{1,2,0:T(8,128)S(1)}, f32[8,512,64]{1,2,0:T(8,128)}, u32[]{:S(2)}) copy-start(f32[8,512,64]{1,2,0:T(8,128)} %get-tuple-element.94) | copy-start | bytes 3145732
  297.3 19.1 %copy-start.11 = (f32[8,512,64]{1,2,0:T(8,128)S(1)}, f32[8,512,64]{1,2,0:T(8,128)}, u32[]{:S(2)}) copy-start(f32[8,512,64]{1,2,0:T(8,128)} %get-tuple-element.78) | copy-start | bytes 3145732
  322.9 4.4 copy-start.16
  327.2 57.3 %copy-start.15 = (bf16[2048,512]{1,0:T(8,128)(2,1)S(1)}, bf16[2048,512]{1,0:T(8,128)(2,1)}, u32[]{:S(2)}) copy-start(bf16[2048,512]{1,0:T(8,128)(2,1)} %get-tuple-element.109) | copy-start | bytes 6291460
  327.2 57.3 %copy-start.19 = (f32[1,2048]{1,0:T(1,128)S(1)}, f32[1,2048]{1,0:T(1,128)}, u32[]{:S(2)}) copy-start(f32[1,2048]{1,0:T(1,128)} %get-tuple-element.211) | copy-start | bytes 24580
  327.2 55.2 %all-gather.8.cloned.1.call-start = ((), (), s32[]{:S(2)}) async-start(), calls=%async_computation.7 | async-start | bytes 2621440 | tf_op jit(solution)/shard_map/all_gather | solution.py:41
  359.7 345.9 %reduce-scatter.6.cloned.1.call-start = ((), (), s32[]{:S(2)}) async-start(), calls=%async_computation.5 | async-start | bytes 2621440 | tf_op jit(solution)/shard_map/reduce_scatter | solution.py:91
  384.5 9.5 copy-start.17
  389.1 94.6 %collective-permute-start.7 = (bf16[1024,512]{1,0:T(8,128)(2,1)S(1)}, bf16[1024,512]{1,0:T(8,128)(2,1)}, u32[]{:S(2)}, u32[]{:S(2)}) collective-permute-start(bf16[1024,512]{1,0:T(8,128)(2,1)S(1)} %multiply_convert_fusion.1), channel_id=1, source_target_pairs={{16,0},{20,4},{24,8},{28,12},{0,16},{4,20},{8,24},{12,28},{17,1},{... | collective-permute-start | bytes 3145736 | tf_op jit(solution)/shard_map/ppermute | solution.py:19
  391.6 137.8 %collective-permute-start.8 = (bf16[1024,512]{1,0:T(8,128)(2,1)S(1)}, bf16[1024,512]{1,0:T(8,128)(2,1)S(1)}, u32[]{:S(2)}, u32[]{:S(2)}) collective-permute-start(bf16[1024,512]{1,0:T(8,128)(2,1)S(1)} %multiply_convert_fusion.1), channel_id=1, source_target_pairs={{20,0},{24,4},{28,8},{0,12},{4,16},{8,20},{12,24},{16,28},{21,1},{... | collective-permute-start | bytes 3145736 | tf_op jit(solution)/shard_map/ppermute | solution.py:19
  394.1 135.4 %collective-permute-start.9 = (bf16[1024,512]{1,0:T(8,128)(2,1)S(1)}, bf16[1024,512]{1,0:T(8,128)(2,1)S(1)}, u32[]{:S(2)}, u32[]{:S(2)}) collective-permute-start(bf16[1024,512]{1,0:T(8,128)(2,1)S(1)} %multiply_convert_fusion.1), channel_id=1, source_target_pairs={{24,0},{28,4},{0,8},{4,12},{8,16},{12,20},{16,24},{20,28},{25,1},{... | collective-permute-start | bytes 3145736 | tf_op jit(solution)/shard_map/ppermute | solution.py:19
  395.3 134.3 %collective-permute-start.10 = (bf16[1024,512]{1,0:T(8,128)(2,1)S(1)}, bf16[1024,512]{1,0:T(8,128)(2,1)S(1)}, u32[]{:S(2)}, u32[]{:S(2)}) collective-permute-start(bf16[1024,512]{1,0:T(8,128)(2,1)S(1)} %multiply_convert_fusion.1), channel_id=1, source_target_pairs={{28,0},{0,4},{4,8},{8,12},{12,16},{16,20},{20,24},{24,28},{29,1},{... | collective-permute-start | bytes 3145736 | tf_op jit(solution)/shard_map/ppermute | solution.py:19
  396.3 133.4 %collective-permute-start.11 = (bf16[1024,512]{1,0:T(8,128)(2,1)S(1)}, bf16[1024,512]{1,0:T(8,128)(2,1)S(1)}, u32[]{:S(2)}, u32[]{:S(2)}) collective-permute-start(bf16[1024,512]{1,0:T(8,128)(2,1)S(1)} %multiply_convert_fusion.1), channel_id=1, source_target_pairs={{4,0},{8,4},{12,8},{16,12},{20,16},{24,20},{28,24},{0,28},{5,1},{9... | collective-permute-start | bytes 3145736 | tf_op jit(solution)/shard_map/ppermute | solution.py:19
  483.7 46.2 %collective-permute-start.12 = (bf16[1024,512]{1,0:T(8,128)(2,1)S(1)}, bf16[1024,512]{1,0:T(8,128)(2,1)S(1)}, u32[]{:S(2)}, u32[]{:S(2)}) collective-permute-start(bf16[1024,512]{1,0:T(8,128)(2,1)S(1)} %multiply_convert_fusion.1), channel_id=1, source_target_pairs={{8,0},{12,4},{16,8},{20,12},{24,16},{28,20},{0,24},{4,28},{9,1},{1... | collective-permute-start | bytes 3145736 | tf_op jit(solution)/shard_map/ppermute | solution.py:19
  529.4 44.2 %collective-permute-start.13 = (bf16[1024,512]{1,0:T(8,128)(2,1)S(1)}, bf16[1024,512]{1,0:T(8,128)(2,1)S(1)}, u32[]{:S(2)}, u32[]{:S(2)}) collective-permute-start(bf16[1024,512]{1,0:T(8,128)(2,1)S(1)} %multiply_convert_fusion.1), channel_id=1, source_target_pairs={{12,0},{16,4},{20,8},{24,12},{28,16},{0,20},{4,24},{8,28},{13,1},{... | collective-permute-start | bytes 3145736 | tf_op jit(solution)/shard_map/ppermute | solution.py:19
  645.6 18.8 %copy-start.5 = (f32[8,512,64]{1,2,0:T(8,128)S(1)}, f32[8,512,64]{1,2,0:T(8,128)}, u32[]{:S(2)}) copy-start(f32[8,512,64]{1,2,0:T(8,128)} %get-tuple-element.70) | copy-start | bytes 3145732
  645.6 18.8 %copy-start.6 = (f32[8,512,64]{1,2,0:T(8,128)S(1)}, f32[8,512,64]{1,2,0:T(8,128)}, u32[]{:S(2)}) copy-start(f32[8,512,64]{1,2,0:T(8,128)} %get-tuple-element.71) | copy-start | bytes 3145732
  645.6 18.8 %copy-start.7 = (f32[8,512,64]{1,2,0:T(8,128)S(1)}, f32[8,512,64]{1,2,0:T(8,128)}, u32[]{:S(2)}) copy-start(f32[8,512,64]{1,2,0:T(8,128)} %get-tuple-element.93) | copy-start | bytes 3145732
  645.6 18.8 %copy-start.12 = (f32[8,512,64]{1,2,0:T(8,128)S(1)}, f32[8,512,64]{1,2,0:T(8,128)}, u32[]{:S(2)}) copy-start(f32[8,512,64]{1,2,0:T(8,128)} %get-tuple-element.64) | copy-start | bytes 3145732
  670.8 34.7 %copy-start.1 = (bf16[512,512]{0,1:T(8,128)(2,1)S(1)}, bf16[512,512]{0,1:T(8,128)(2,1)}, u32[]{:S(2)}) copy-start(bf16[512,512]{0,1:T(8,128)(2,1)} %fusion.271) | copy-start | bytes 1572868
  675.1 57.3 %copy-start.14 = (bf16[2048,512]{1,0:T(8,128)(2,1)S(1)}, bf16[2048,512]{1,0:T(8,128)(2,1)}, u32[]{:S(2)}) copy-start(bf16[2048,512]{1,0:T(8,128)(2,1)} %get-tuple-element.107) | copy-start | bytes 6291460
  675.1 55.2 %all-gather.10.cloned.1.call-start = ((), (), s32[]{:S(2)}) async-start(), calls=%async_computation.8 | async-start | bytes 2621440 | tf_op jit(solution)/shard_map/all_gather | solution.py:41
  707.6 347.8 %reduce-scatter.8.cloned.1.call-start = ((), (), s32[]{:S(2)}) async-start(), calls=%async_computation.6 | async-start | bytes 2621440 | tf_op jit(solution)/shard_map/reduce_scatter | solution.py:91
  738.0 94.6 %collective-permute-start.14 = (bf16[1024,512]{1,0:T(8,128)(2,1)}, bf16[1024,512]{1,0:T(8,128)(2,1)S(1)}, u32[]{:S(2)}, u32[]{:S(2)}) collective-permute-start(bf16[1024,512]{1,0:T(8,128)(2,1)} %multiply_convert_fusion), channel_id=1, source_target_pairs={{16,0},{20,4},{24,8},{28,12},{0,16},{4,20},{8,24},{12,28},{17,1},{... | collective-permute-start | bytes 3145736 | tf_op jit(solution)/shard_map/ppermute | solution.py:19
  740.4 138.0 %collective-permute-start.15 = (bf16[1024,512]{1,0:T(8,128)(2,1)}, bf16[1024,512]{1,0:T(8,128)(2,1)S(1)}, u32[]{:S(2)}, u32[]{:S(2)}) collective-permute-start(bf16[1024,512]{1,0:T(8,128)(2,1)} %multiply_convert_fusion), channel_id=1, source_target_pairs={{20,0},{24,4},{28,8},{0,12},{4,16},{8,20},{12,24},{16,28},{21,1},{... | collective-permute-start | bytes 3145736 | tf_op jit(solution)/shard_map/ppermute | solution.py:19
  742.9 135.6 %collective-permute-start.16 = (bf16[1024,512]{1,0:T(8,128)(2,1)}, bf16[1024,512]{1,0:T(8,128)(2,1)S(1)}, u32[]{:S(2)}, u32[]{:S(2)}) collective-permute-start(bf16[1024,512]{1,0:T(8,128)(2,1)} %multiply_convert_fusion), channel_id=1, source_target_pairs={{24,0},{28,4},{0,8},{4,12},{8,16},{12,20},{16,24},{20,28},{25,1},{... | collective-permute-start | bytes 3145736 | tf_op jit(solution)/shard_map/ppermute | solution.py:19
  744.0 134.5 %collective-permute-start.17 = (bf16[1024,512]{1,0:T(8,128)(2,1)}, bf16[1024,512]{1,0:T(8,128)(2,1)S(1)}, u32[]{:S(2)}, u32[]{:S(2)}) collective-permute-start(bf16[1024,512]{1,0:T(8,128)(2,1)} %multiply_convert_fusion), channel_id=1, source_target_pairs={{28,0},{0,4},{4,8},{8,12},{12,16},{16,20},{20,24},{24,28},{29,1},{... | collective-permute-start | bytes 3145736 | tf_op jit(solution)/shard_map/ppermute | solution.py:19
  745.1 134.9 %collective-permute-start.18 = (bf16[1024,512]{1,0:T(8,128)(2,1)}, bf16[1024,512]{1,0:T(8,128)(2,1)S(1)}, u32[]{:S(2)}, u32[]{:S(2)}) collective-permute-start(bf16[1024,512]{1,0:T(8,128)(2,1)} %multiply_convert_fusion), channel_id=1, source_target_pairs={{4,0},{8,4},{12,8},{16,12},{20,16},{24,20},{28,24},{0,28},{5,1},{9... | collective-permute-start | bytes 3145736 | tf_op jit(solution)/shard_map/ppermute | solution.py:19
  832.6 47.5 %collective-permute-start.19 = (bf16[1024,512]{1,0:T(8,128)(2,1)}, bf16[1024,512]{1,0:T(8,128)(2,1)S(1)}, u32[]{:S(2)}, u32[]{:S(2)}) collective-permute-start(bf16[1024,512]{1,0:T(8,128)(2,1)} %multiply_convert_fusion), channel_id=1, source_target_pairs={{8,0},{12,4},{16,8},{20,12},{24,16},{28,20},{0,24},{4,28},{9,1},{1... | collective-permute-start | bytes 3145736 | tf_op jit(solution)/shard_map/ppermute | solution.py:19
  878.4 44.2 %collective-permute-start.20 = (bf16[1024,512]{1,0:T(8,128)(2,1)}, bf16[1024,512]{1,0:T(8,128)(2,1)S(1)}, u32[]{:S(2)}, u32[]{:S(2)}) collective-permute-start(bf16[1024,512]{1,0:T(8,128)(2,1)} %multiply_convert_fusion), channel_id=1, source_target_pairs={{12,0},{16,4},{20,8},{24,12},{28,16},{0,20},{4,24},{8,28},{13,1},{... | collective-permute-start | bytes 3145736 | tf_op jit(solution)/shard_map/ppermute | solution.py:19
  994.8 18.8 %copy-start.8 = (f32[8,512,64]{1,2,0:T(8,128)S(1)}, f32[8,512,64]{1,2,0:T(8,128)}, u32[]{:S(2)}) copy-start(f32[8,512,64]{1,2,0:T(8,128)} %get-tuple-element.56) | copy-start | bytes 3145732
  994.8 18.8 %copy-start.9 = (f32[8,512,64]{1,2,0:T(8,128)S(1)}, f32[8,512,64]{1,2,0:T(8,128)}, u32[]{:S(2)}) copy-start(f32[8,512,64]{1,2,0:T(8,128)} %get-tuple-element.57) | copy-start | bytes 3145732
  994.8 18.8 %copy-start.10 = (f32[8,512,64]{1,2,0:T(8,128)S(1)}, f32[8,512,64]{1,2,0:T(8,128)}, u32[]{:S(2)}) copy-start(f32[8,512,64]{1,2,0:T(8,128)} %get-tuple-element.92) | copy-start | bytes 3145732
  994.8 18.8 %copy-start.13 = (f32[8,512,64]{1,2,0:T(8,128)S(1)}, f32[8,512,64]{1,2,0:T(8,128)}, u32[]{:S(2)}) copy-start(f32[8,512,64]{1,2,0:T(8,128)} %get-tuple-element.50) | copy-start | bytes 3145732
  1020.0 35.4 %copy-start = (bf16[512,512]{0,1:T(8,128)(2,1)S(1)}, bf16[512,512]{0,1:T(8,128)(2,1)}, u32[]{:S(2)}) copy-start(bf16[512,512]{0,1:T(8,128)(2,1)} %add_convert_fusion.4) | copy-start | bytes 1572868
Sparse Core Ops, SparseCore 0:
  8.9 25.2 all-gather.5
  327.4 30.2 reduce-scatter.3
  359.8 22.5 all-gather.7
  675.2 30.2 reduce-scatter.5
  707.7 22.5 all-gather.9
  1024.4 30.9 reduce-scatter.7
where the time goes:
time: 1070 us; the launch traced here: 1060 us
  waiting for transfers between devices  658 us (61%)
  other arithmetic  298 us (28%)
  matrix products  38.5 us (4%)
  starting transfers between devices  29.4 us (3%)
  local copies, waits for them, and re-layouts  25.7 us (2%)
  between operations  14.7 us (1%)
    ppermute x21, waiting for transfers between devices, from_behind(): return lax.ppermute(block, axis, route)  504 us
    dot_general x12, other arithmetic, body(): jnp.einsum('shc,shdc->hdc', weights[offset], shifted, preferred_element_t...  137 us
    dot_general x6, other arithmetic, body(): jnp.einsum('hdc,shdc->shc', query_heads, shifted, preferred_element_type=...  116 us
    reduce_scatter x3, waiting for transfers between devices, body(): lax.psum_scatter(lax.dot_general(w_layer, mixed_out, (((0,), (0,)), ((),...  91.6 us
    all_gather x3, waiting for transfers between devices, body(): lax.all_gather(current, 'tp', axis=1, tiled=True)[0].astype(jnp.float32)  61.9 us
    ppermute x21, starting transfers between devices, from_behind(): return lax.ppermute(block, axis, route)  29.2 us
  transfers between devices with their start and end apart: 27, of which 15 were waited for; matrix products, arithmetic and copies ran while one was open for 3% of the time, Pallas kernels for 0%

commit v1 on v0

v1 whole, which is shorter than its diff:
```python
import functools
import math

import jax
import jax.numpy as jnp
from jax import lax
from jax.experimental import pallas as pl
from jax.experimental.pallas import tpu as pltpu
from jax.sharding import PartitionSpec as P

HEAD_DIM = 64
WIN_R = 8
WIN_C = 16
HALF_R = WIN_R // 2
HALF_C = WIN_C // 2
EPS = 1e-06
LOG2E = math.log2(math.e)
Q_SCALE = HEAD_DIM ** (-0.5) * LOG2E
MASKED = -1e30
BLOCK = 128
F32 = jnp.float32
BF16 = jnp.bfloat16


def _permute_kernel(x_ref, o_ref, *, rows, cols):
    tokens = rows * cols
    out_at = lax.broadcasted_iota(jnp.int32, (tokens, tokens), 0)
    in_at = lax.broadcasted_iota(jnp.int32, (tokens, tokens), 1)
    pick = (out_at % rows) * cols + out_at // rows == in_at
    o_ref[...] = jnp.dot(
        pick.astype(F32).astype(BF16), x_ref[...], preferred_element_type=F32
    ).astype(BF16)


def permute_tokens(x, rows, cols):
    return pl.pallas_call(
        functools.partial(_permute_kernel, rows=rows, cols=cols),
        out_shape=jax.ShapeDtypeStruct(x.shape, BF16),
        name="to_column_order",
    )(x)


def _qkv_kernel(ids_ref, *refs, n_parts, halo, d_model):
    parts = refs[:n_parts]
    gain_ref, wq_ref, wk_ref, wv_ref = refs[n_parts : n_parts + 4]
    q_ref, k_ref, v_ref, first_ref, last_ref = refs[n_parts + 4 : n_parts + 9]
    scaled_ref, inverse_ref = refs[n_parts + 9 :]
    tokens, chunk = parts[0].shape

    @pl.when(pl.program_id(0) == 0)
    def _():
        squares = jnp.zeros((tokens, 128), F32)
        for at, part in enumerate(parts):
            wide = part[...].astype(F32)
            where = ids_ref[at]
            scaled_ref[where] = (wide * gain_ref[0, where]).astype(BF16)
            for lane in range(0, chunk, 128):
                tile = wide[:, lane : lane + 128]
                squares = squares + tile * tile
        total = jnp.sum(squares, axis=1, keepdims=True)
        inverse_ref[...] = lax.rsqrt(total / d_model + EPS)

    scaled = jnp.concatenate([scaled_ref[at] for at in range(n_parts)], axis=1)
    inverse = inverse_ref[...]
    k = (jnp.dot(scaled, wk_ref[0], preferred_element_type=F32) * inverse).astype(BF16)
    k_ref[...] = k
    v = (jnp.dot(scaled, wv_ref[0], preferred_element_type=F32) * inverse).astype(BF16)
    v_ref[...] = v
    first_ref[0] = k[:halo]
    first_ref[1] = v[:halo]
    last_ref[0] = k[tokens - halo :]
    last_ref[1] = v[tokens - halo :]
    q = jnp.dot(scaled, wq_ref[0], preferred_element_type=F32) * (inverse * Q_SCALE)
    q_ref[...] = q.astype(BF16)


def qkv(layer, parts, ids, gains, w_query, w_key, w_value, halo):
    tokens, chunk = parts[0].shape
    n_parts = len(parts)
    d_model = n_parts * chunk
    channels = w_query.shape[2]
    tile = min(256, channels)
    whole = pl.BlockSpec((tokens, chunk), lambda j, ids: (0, 0))
    weight = pl.BlockSpec((1, d_model, tile), lambda j, ids: (layer, 0, j))
    out_tile = pl.BlockSpec((tokens, tile), lambda j, ids: (0, j))
    edge = pl.BlockSpec((2, halo, tile), lambda j, ids: (0, 0, j))
    out = jax.ShapeDtypeStruct((tokens, channels), BF16)
    edge_out = jax.ShapeDtypeStruct((2, halo, channels), BF16)
    return pl.pallas_call(
        functools.partial(_qkv_kernel, n_parts=n_parts, halo=halo, d_model=d_model),
        grid_spec=pltpu.PrefetchScalarGridSpec(
            num_scalar_prefetch=1,
            grid=(channels // tile,),
            in_specs=[whole] * n_parts
            + [pl.BlockSpec((1, n_parts, 1, chunk), lambda j, ids: (layer, 0, 0, 0))]
            + [weight] * 3,
            out_specs=[out_tile] * 3 + [edge] * 2,
            scratch_shapes=[
                pltpu.VMEM((n_parts, tokens, chunk), BF16),
                pltpu.VMEM((tokens, 1), F32),
            ],
        ),
        out_shape=[out] * 3 + [edge_out] * 2,
        name="qkv",
    )(ids, *parts, gains, w_query, w_key, w_value)


def _attention_kernel(
    q_ref, k_ref, v_ref, before_ref, after_ref, base_ref, o_ref, k_all, v_all, bias_ref, *, rows
):
    tokens = q_ref.shape[0]
    halo = before_ref.shape[1]
    window = base_ref.shape[3]
    k_all[:halo] = before_ref[0]
    v_all[:halo] = before_ref[1]
    k_all[halo : halo + tokens] = k_ref[...]
    v_all[halo : halo + tokens] = v_ref[...]
    k_all[halo + tokens :] = after_ref[0]
    v_all[halo + tokens :] = after_ref[1]
    for head in range(2):
        base = base_ref[0, head]
        for col in range(BLOCK // rows):
            shifted = base if col == 0 else pltpu.roll(base, col * rows, 1)
            bias_ref[head * BLOCK + col * rows : head * BLOCK + (col + 1) * rows] = shifted
    low = lax.broadcasted_iota(jnp.int32, (BLOCK, 2 * HEAD_DIM), 1) < HEAD_DIM
    ones = jnp.ones((window, 2 * HEAD_DIM), BF16)
    for at in range(0, tokens, BLOCK):
        q = q_ref[at : at + BLOCK].astype(F32)
        both = jnp.concatenate([jnp.where(low, q, 0.0), jnp.where(low, 0.0, q)], axis=0)
        keys = k_all[at : at + window]
        scores = lax.dot_general(
            both.astype(BF16), keys, (((1,), (1,)), ((), ())), preferred_element_type=F32
        )
        scores = scores + bias_ref[...]
        highest = jnp.max(scores, axis=1, keepdims=True)
        weights = jnp.exp2(scores - highest).astype(BF16)
        values = jnp.concatenate([v_all[at : at + window], ones], axis=1)
        mixed = jnp.dot(weights, values, preferred_element_type=F32)
        width = 2 * HEAD_DIM
        top = jnp.where(low, mixed[:BLOCK, :width], mixed[BLOCK:, :width])
        total = jnp.where(low, mixed[:BLOCK, width:], mixed[BLOCK:, width:])
        o_ref[at : at + BLOCK] = (top / total).astype(BF16)


def attention(layer, q, k, v, before, after, bases, rows):
    tokens, channels = q.shape
    halo = before.shape[1]
    window = bases.shape[3]
    width = 2 * HEAD_DIM
    pair = pl.BlockSpec((tokens, width), lambda p: (0, p))
    edge = pl.BlockSpec((2, halo, width), lambda p: (0, 0, p))
    return pl.pallas_call(
        functools.partial(_attention_kernel, rows=rows),
        grid=(channels // width,),
        in_specs=[pair] * 3
        + [edge] * 2
        + [pl.BlockSpec((1, 2, rows, window), lambda p: (layer, p, 0, 0))],
        out_specs=pair,
        scratch_shapes=[
            pltpu.VMEM((tokens + 2 * halo, width), BF16),
            pltpu.VMEM((tokens + 2 * halo, width), BF16),
            pltpu.VMEM((2 * BLOCK, window), F32),
        ],
        out_shape=jax.ShapeDtypeStruct((tokens, channels), BF16),
        name="attention",
    )(q, k, v, before, after, bases)


def _project_kernel(id_ref, own_ref, other_ref, w_own_ref, w_other_ref, o_ref):
    acc = jnp.dot(own_ref[...], w_own_ref[0], preferred_element_type=F32)
    acc = acc + jnp.dot(other_ref[...], w_other_ref[0], preferred_element_type=F32)
    o_ref[...] = acc.astype(BF16)


def project(layer, own, other, w_out, w_other, chunk_id):
    tokens, channels = own.shape
    chunk = w_other.shape[2]
    tile = min(256, chunk)
    steps = chunk // tile
    mixed = pl.BlockSpec((tokens, channels), lambda j, at: (0, 0))
    return pl.pallas_call(
        _project_kernel,
        grid_spec=pltpu.PrefetchScalarGridSpec(
            num_scalar_prefetch=1,
            grid=(steps,),
            in_specs=[
                mixed,
                mixed,
                pl.BlockSpec((1, channels, tile), lambda j, at: (layer, 0, at[0] * steps + j)),
                pl.BlockSpec((1, channels, tile), lambda j, at: (layer, 0, j)),
            ],
            out_specs=pl.BlockSpec((tokens, tile), lambda j, at: (0, j)),
        ),
        out_shape=jax.ShapeDtypeStruct((tokens, chunk), BF16),
        name="project",
    )(chunk_id, own, other, w_out, w_other)


def _finish_kernel(x_ref, *refs, rows, cols):
    o_ref = refs[-1]
    tokens = rows * cols
    update = refs[0][...].astype(F32)
    for ref in refs[1:-1]:
        update = update + ref[...].astype(F32)
    grid = (x_ref[...].astype(F32) + update).astype(BF16)
    out_at = lax.broadcasted_iota(jnp.int32, (tokens, tokens), 0)
    in_at = lax.broadcasted_iota(jnp.int32, (tokens, tokens), 1)
    pick = (out_at % cols) * rows + out_at // cols == in_at
    o_ref[...] = jnp.dot(
        pick.astype(F32).astype(BF16), grid, preferred_element_type=F32
    ).astype(BF16)


def finish(x, partials, rows, cols):
    return pl.pallas_call(
        functools.partial(_finish_kernel, rows=rows, cols=cols),
        out_shape=jax.ShapeDtypeStruct(x.shape, BF16),
        name="to_row_order",
    )(x, *partials)


def ring_order(mesh):
    n_sp = mesh.shape["sp"]
    at = list(mesh.axis_names).index("sp")
    devices = mesh.devices if at == 0 else mesh.devices.T
    try:
        places = [tuple(devices[i].flat[0].coords) for i in range(n_sp)]
    except Exception:
        return list(range(n_sp))
    xs = sorted({p[0] for p in places})
    zs = sorted({p[2] for p in places})
    index = {(p[0], p[2]): i for i, p in enumerate(places)}
    if len(index) != n_sp or len(xs) * len(zs) != n_sp:
        return list(range(n_sp))
    path = [(xs[0], z) for z in zs]
    for turn, z in enumerate(reversed(zs)):
        line = xs[1:] if turn % 2 == 0 else xs[1:][::-1]
        path += [(x, z) for x in line]
    return [index[p] for p in path]


def dense_bias(rel_bias, rows, window):
    layers, heads = rel_bias.shape[:2]
    span = WIN_C * rows
    slot = lax.broadcasted_iota(jnp.int32, (WIN_R * WIN_C, rows * span), 0)
    place = lax.broadcasted_iota(jnp.int32, (WIN_R * WIN_C, rows * span), 1)
    row_slot = (place % rows - place // span + HALF_R) % rows
    col_slot = (place % span) // rows
    pick = (slot // WIN_C == row_slot) & (slot % WIN_C == col_slot)
    flat = rel_bias.reshape(layers * heads, WIN_R * WIN_C) * LOG2E
    base = jnp.dot(flat, pick.astype(F32), precision=lax.Precision.HIGHEST)
    base = jnp.where(row_slot[:1] < WIN_R, base, MASKED)
    base = base.reshape(layers, heads, rows, span)
    return jnp.pad(base, ((0, 0),) * 3 + ((0, window - span),), constant_values=MASKED)


def body(
    token_grid, norm_gain, w_query, w_key, w_value, w_out, rel_bias, *, order
):
    n_sp = lax.axis_size("sp")
    n_tp = lax.axis_size("tp")
    n_y = n_tp // 2
    layers = norm_gain.shape[0]
    chunk = token_grid.shape[1]
    rows = n_sp * token_grid.shape[0]
    cols = token_grid.shape[2] // n_sp
    tokens = rows * cols
    halo = HALF_C * rows
    window = BLOCK + 2 * halo
    here = lax.axis_index("tp")
    my_y, my_core = here // 2, here % 2
    rank = [order.index(i) for i in range(n_sp)]
    after_of = [(order[i], order[(i + 1) % n_sp]) for i in range(n_sp)]
    before_of = [(b, a) for a, b in after_of]

    def over_core(x):
        return lax.ppermute(x, "tp", [(i, i ^ 1) for i in range(n_tp)])

    def over_y(x, shift):
        return lax.ppermute(x, "tp", [(i, (i + 2 * shift) % n_tp) for i in range(n_tp)])

    blocks = token_grid[0].T.reshape(n_sp, cols, chunk)
    blocks = jnp.stack([blocks[rank[i]] for i in range(n_sp)])
    mine = lax.all_to_all(blocks, "sp", 0, 0, tiled=True).reshape(tokens, chunk)
    mine = permute_tokens(mine, rows, cols)

    w_others = []
    for y in range(n_y):
        theirs = lax.dynamic_slice_in_dim(w_out, (2 * y + 1 - my_core) * chunk, chunk, 2)
        w_others.append(over_core(theirs))
    gains = norm_gain.astype(F32).reshape(layers, n_tp, 1, chunk)
    bases = dense_bias(rel_bias, rows, window)

    own = [mine] + [over_y(mine, shift) for shift in range(1, n_y)]
    ys = [(my_y - shift) % n_y for shift in range(n_y)]
    grids = own
    for layer in range(layers):
        other = [over_core(x) for x in grids]
        ids = jnp.stack([2 * y + my_core for y in ys] + [2 * y + 1 - my_core for y in ys])
        q, k, v, first, last = qkv(
            layer, grids + other, ids.astype(jnp.int32), gains, w_query, w_key, w_value, halo
        )
        after = lax.ppermute(first, "sp", before_of)
        before = lax.ppermute(last, "sp", after_of)
        mixed = attention(layer, q, k, v, before, after, bases, rows)
        mixed_other = over_core(mixed)

        def partial_of(y, w_other):
            chunk_id = (2 * y + my_core).astype(jnp.int32).reshape(1)
            return project(layer, mixed, mixed_other, w_out, w_other, chunk_id)

        if layer == 0:
            absolute = []
            for y in range(n_y):
                pick = own[0]
                for shift in range(1, n_y):
                    pick = jnp.where(ys[shift] == y, own[shift], pick)
                absolute.append(pick)
            grids = absolute
            ys = [jnp.int32(y) for y in range(n_y)]
        if layer + 1 < layers:
            fresh = []
            for y in range(n_y):
                partial = partial_of(jnp.int32(y), w_others[y])
                update = partial.astype(F32)
                for shift in range(1, n_y):
                    update = update + over_y(partial, shift).astype(F32)
                fresh.append((grids[y].astype(F32) + update).astype(BF16))
            grids = fresh
        else:
            def select(arrays, y):
                pick = arrays[0]
                for at in range(1, n_y):
                    pick = jnp.where(y == at, arrays[at], pick)
                return pick

            partials = []
            for shift in list(range(1, n_y)) + [0]:
                y = (my_y + shift) % n_y
                partial = partial_of(y, select(w_others, y))
                partials.append(partial if shift == 0 else over_y(partial, shift))
            done = finish(select(grids, my_y), partials[::-1], rows, cols)

    sent = lax.all_to_all(done.reshape(n_sp, cols, chunk), "sp", 0, 0, tiled=True)
    sent = jnp.stack([sent[order[i]] for i in range(n_sp)])
    return sent.reshape(n_sp * cols, chunk).T[None]


def solution(mesh):
    in_specs = (
        P("sp", "tp", None),
        P(),
        P(None, None, "tp"),
        P(None, None, "tp"),
        P(None, None, "tp"),
        P(None, "tp", None),
        P(None, "tp", None, None),
    )
    out_specs = P("sp", "tp", None)
    return jax.shard_map(
        functools.partial(body, order=ring_order(mesh)),
        mesh=mesh,
        in_specs=in_specs,
        out_specs=out_specs,
        check_vma=False,
    )
```

time: 1070 us -> 226 us (0.21)
  waiting for transfers between devices: 658 us -> 92.1 us
  other arithmetic: 298 us -> 7.39 us
  Pallas kernels: 0 us -> 65.4 us
  matrix products: 38.5 us -> 0.38 us
  blocking collectives: 0 us -> 17.9 us
  between operations: 14.7 us -> 0.28 us
    ppermute x21 -> x23, waiting for transfers between devices: 504 us -> 82.8 us  [the longest x6 60.1 us: over_y(): lax.ppermute(x, 'tp', [(i, (i + 2 * shift) % n_tp) for i in range(n_tp)])]
    dot_general x18 -> x0, other arithmetic: 253 us -> none  [the longest x12 137 us: body(): jnp.einsum('shc,shdc->hdc', weights[offset], shifted, preferred_element_t...]
    reduce_scatter x3 -> x0, waiting for transfers between devices: 91.6 us -> none  [body(): lax.psum_scatter(lax.dot_general(w_layer, mixed_out, (((0,), (0,)), ((),...]
    pallas_call x0 -> x14, Pallas kernels: none -> 65.4 us  [the longest x3 26.5 us: qkv(): pl.pallas_call(functools.partial(_qkv_kernel, n_parts=n_parts, halo=halo,...]
    all_gather x3 -> x0, waiting for transfers between devices: 61.9 us -> none  [body(): lax.all_gather(current, 'tp', axis=1, tiled=True)[0].astype(jnp.float32)]
    dot_general x9 -> x1, matrix products: 38.5 us -> 0.38 us  [dense_bias(): base = jnp.dot(flat, pick.astype(F32), precision=lax.Precision.HIGHEST)]
    convert_element_type x9 -> x1, other arithmetic: 25.6 us -> 1.65 us  [body(): fresh.append((grids[y].astype(F32) + update).astype(BF16))]
    all_to_all x0 -> x1, blocking collectives: none -> 17.9 us  [body(): lax.all_to_all(done.reshape(n_sp, cols, chunk), 'sp', 0, 0, tiled=True)]
  transfers between devices with their start and end apart: 27 -> 24, of which waited for: 15 -> 20; matrix products, arithmetic and copies ran while one was open for 3% -> 4% of each run, Pallas kernels for 0% -> 13%
where the time goes in v1:
time: 226 us; the launch traced here: 225 us
  waiting for transfers between devices  92.1 us (41%)
  Pallas kernels  65.4 us (29%)
  starting transfers between devices  22.4 us (10%)
  local copies, waits for them, and re-layouts  19.4 us (9%)
  blocking collectives  17.9 us (8%)
  other arithmetic  7.39 us (3%)
    ppermute x6, waiting for transfers between devices, over_y(): lax.ppermute(x, 'tp', [(i, (i + 2 * shift) % n_tp) for i in range(n_tp)])  60.1 us
    pallas_call x3, Pallas kernels, qkv(): pl.pallas_call(functools.partial(_qkv_kernel, n_parts=n_parts, halo=halo,...  26.5 us
    pallas_call x6, Pallas kernels, project(): pl.pallas_call(_project_kernel, grid_spec=pltpu.PrefetchScalarGridSpec(nu...  18.3 us
    all_to_all x1, blocking collectives, body(): lax.all_to_all(done.reshape(n_sp, cols, chunk), 'sp', 0, 0, tiled=True)  17.9 us
    pallas_call x3, Pallas kernels, attention(): pl.pallas_call(functools.partial(_attention_kernel, rows=rows), grid=(cha...  15.6 us
    unnamed x71, local copies, waits for them, and re-layouts  12.2 us
    ppermute x3, waiting for transfers between devices, body(): before = lax.ppermute(last, 'sp', after_of)  10.3 us
    ppermute x11, waiting for transfers between devices, over_core(): return lax.ppermute(x, 'tp', [(i, i ^ 1) for i in range(n_tp)])  9.8 us
  transfers between devices with their start and end apart: 24, of which 20 were waited for; matrix products, arithmetic and copies ran while one was open for 4% of the time, Pallas kernels for 13%

profile of v1, /device:TPU:0, one launch (start us, length us, event | category | flops | bytes accessed | tf_op | source)
XLA Modules:
  0.0 225.2 jit_solution(1387474806763970558)
XLA Ops:
  0.0 1.3 copy.12
  1.3 0.6 fusion.31
  1.9 0.6 fusion.30
  2.5 0.6 fusion.29
  3.2 0.6 fusion.28
  3.8 0.6 fusion.27
  6.3 7.3 %all-to-all-start = ((bf16[8,64,512]{2,1,0:T(8,128)(2,1)}), bf16[8,64,512]{2,1,0:T(8,128)(2,1)}, u32[]{:S(2)}, u32[]{:S(2)}) async-start(bf16[8,64,512]{2,1,0:T(8,128)(2,1)} %fusion.24), calls=%async_computation | async-start | bytes 1048576 | tf_op jit(solution)/shard_map/all_to_all | solution.py:284
  13.6 4.0 %constant_dynamic-slice_fusion.1 = (bf16[3,512,512]{2,1,0:T(8,128)(2,1)}, bf16[3,512,512]{2,1,0:T(8,128)(2,1)}) fusion(bf16[3,512,2048]{2,1,0:T(8,128)(2,1)} %w_own_ref.11, s32[]{:T(128)S(6)} %select_n.119, s32[]{:T(128)S(6)} %select_n.122), kind=kLoop, calls=%fused_computation.91 | loop fusion | bytes 6291464 | tf_op jit(solution)/shard_map/dynamic_slice | solution.py:289
  18.2 0.7 reshape.48.refs_4_
  19.0 9.2 %all-to-all-done = bf16[8,64,512]{2,1,0:T(8,128)(2,1)} async-done(((bf16[8,64,512]{2,1,0:T(8,128)(2,1)}), bf16[8,64,512]{2,1,0:T(8,128)(2,1)}, u32[]{:S(2)}, u32[]{:S(2)}) %all-to-all-start) | async-done | bytes 524320 | tf_op jit(solution)/shard_map/all_to_all | solution.py:284
  28.2 2.3 %to_column_order.1.refs_0_ = bf16[512,512]{1,0:T(8,128)(2,1)} custom-call(bf16[512,512]{1,0:T(8,128)(2,1)} %bitcast.11.x_ref), custom_call_target="tpu_custom_call" | custom-call | tf_op jit(solution)/shard_map/to_column_order/pallas_call | solution.py:36
  30.5 1.5 collective-permute-start
  32.1 10.9 %collective-permute-done.refs_1_ = bf16[512,512]{1,0:T(8,128)(2,1)S(1)} collective-permute-done((bf16[512,512]{1,0:T(8,128)(2,1)}, bf16[512,512]{1,0:T(8,128)(2,1)S(1)}, u32[]{:S(2)}, u32[]{:S(2)}) %collective-permute-start) | collective-permute-done | bytes 524320 | tf_op jit(solution)/shard_map/ppermute | solution.py:280
  43.0 0.8 copy-done.9
  43.8 0.6 pad_add_fusion.ids_ref
  44.6 1.3 collective-permute-done.2.refs_3_
  45.8 8.8 %qkv.3 = (bf16[512,512]{1,0:T(8,128)(2,1)}, bf16[512,512]{1,0:T(8,128)(2,1)}, bf16[512,512]{1,0:T(8,128)(2,1)}, bf16[2,64,512]{2,1,0:T(8,128)(2,1)}, bf16[2,64,512]{2,1,0:T(8,128)(2,1)}) custom-call(s32[4]{0:T(128)} %pad_add_fusion.ids_ref, bf16[512,512]{1,0:T(8,128)(2,1)} %to_column_order.1.refs_0_, bf16[512,512]{1,0:T(8,128)(2,1)} %copy-done.9, ...), custom_call_target="tpu_custom_call" | custom-call | tf_op jit(solution)/shard_map/qkv/pallas_call | solution.py:89
  54.6 2.1 collective-permute-start.4
  57.2 0.7 pad.4.base_ref
  57.9 2.8 %collective-permute-done.3.before_ref = bf16[2,64,512]{2,1,0:T(8,128)(2,1)S(1)} collective-permute-done((bf16[2,64,512]{2,1,0:T(8,128)(2,1)}, bf16[2,64,512]{2,1,0:T(8,128)(2,1)S(1)}, u32[]{:S(2)}, u32[]{:S(2)}) %collective-permute-start.3) | collective-permute-done | bytes 131104 | tf_op jit(solution)/shard_map/ppermute | solution.py:304
  60.7 0.6 copy-done.20
  61.4 5.2 %attention.3.own_ref = bf16[512,512]{1,0:T(8,128)(2,1)} custom-call(bf16[512,512]{1,0:T(8,128)(2,1)} %get-tuple-element.20.q_ref, bf16[512,512]{1,0:T(8,128)(2,1)} %get-tuple-element.21.k_ref, bf16[512,512]{1,0:T(8,128)(2,1)} %get-tuple-element.22.v_ref, bf16[2,64,512]{2,1,0:T(8,128)(2,1)} %copy-done.20, bf16[2,64,512]{2,1,0:T(8,128)(2,1)} %copy-done.21, ...), custom_call_target="tpu_custom_call" | custom-call | tf_op jit(solution)/shard_map/attention/pallas_call | solution.py:152
  66.7 2.2 collective-permute-done.5.other_ref
  68.9 3.1 %project.7 = bf16[512,512]{1,0:T(8,128)(2,1)} custom-call(s32[1]{0:T(128)} %bitcast.17.id_ref, bf16[512,512]{1,0:T(8,128)(2,1)} %attention.3.own_ref, bf16[512,512]{1,0:T(8,128)(2,1)} %collective-permute-done.5.other_ref, bf16[3,512,2048]{2,1,0:T(8,128)(2,1)} %w_own_ref.11, bf16[3,512,512]{2,1,0:T(8,128)(2,1)} %copy-done), custom_call_target="tpu_custom_call" | custom-call | tf_op jit(solution)/shard_map/project/pallas_call | solution.py:181
  72.0 1.5 collective-permute-start.9
  73.5 1.1 copy-done.2
  74.6 3.1 %project.6 = bf16[512,512]{1,0:T(8,128)(2,1)} custom-call(s32[1]{0:T(128)} %bitcast.12.id_ref, bf16[512,512]{1,0:T(8,128)(2,1)} %attention.3.own_ref, bf16[512,512]{1,0:T(8,128)(2,1)} %collective-permute-done.5.other_ref, bf16[3,512,2048]{2,1,0:T(8,128)(2,1)} %w_own_ref.11, bf16[3,512,512]{2,1,0:T(8,128)(2,1)} %copy-done.2), custom_call_target="tpu_custom_call" | custom-call | tf_op jit(solution)/shard_map/project/pallas_call | solution.py:181
  78.3 8.8 %collective-permute-done.9 = bf16[512,512]{1,0:T(8,128)(2,1)} collective-permute-done((bf16[512,512]{1,0:T(8,128)(2,1)}, bf16[512,512]{1,0:T(8,128)(2,1)}, u32[]{:S(2)}, u32[]{:S(2)}) %collective-permute-start.9) | collective-permute-done | bytes 524320 | tf_op jit(solution)/shard_map/ppermute | solution.py:280
  87.1 10.3 %collective-permute-done.7 = bf16[512,512]{1,0:T(8,128)(2,1)S(1)} collective-permute-done((bf16[512,512]{1,0:T(8,128)(2,1)}, bf16[512,512]{1,0:T(8,128)(2,1)S(1)}, u32[]{:S(2)}, u32[]{:S(2)}) %collective-permute-start.7) | collective-permute-done | bytes 524320 | tf_op jit(solution)/shard_map/ppermute | solution.py:280
  97.4 1.7 add_convert_fusion.3
  100.2 0.8 collective-permute-done.10.refs_2_
  101.0 0.7 collective-permute-done.11.refs_3_
  101.8 0.8 copy-done.18
  102.6 8.8 %qkv.4 = (bf16[512,512]{1,0:T(8,128)(2,1)}, bf16[512,512]{1,0:T(8,128)(2,1)}, bf16[512,512]{1,0:T(8,128)(2,1)}, bf16[2,64,512]{2,1,0:T(8,128)(2,1)}, bf16[2,64,512]{2,1,0:T(8,128)(2,1)}) custom-call(s32[4]{0:T(128)} %pad_add_fusion.1.ids_ref, bf16[512,512]{1,0:T(8,128)(2,1)} %copy-done.6, bf16[512,512]{1,0:T(8,128)(2,1)} %copy-done.4, ...), custom_call_target="tpu_custom_call" | custom-call | tf_op jit(solution)/shard_map/qkv/pallas_call | solution.py:89
  111.5 1.5 collective-permute-start.12
  113.5 3.7 %collective-permute-done.12.before_ref = bf16[2,64,512]{2,1,0:T(8,128)(2,1)S(1)} collective-permute-done((bf16[2,64,512]{2,1,0:T(8,128)(2,1)}, bf16[2,64,512]{2,1,0:T(8,128)(2,1)S(1)}, u32[]{:S(2)}, u32[]{:S(2)}) %collective-permute-start.12) | collective-permute-done | bytes 131104 | tf_op jit(solution)/shard_map/ppermute | solution.py:304
  117.3 1.2 collective-permute-done.13.after_ref
  118.4 0.7 copy-done.25
  119.1 5.2 %attention.4.own_ref = bf16[512,512]{1,0:T(8,128)(2,1)} custom-call(bf16[512,512]{1,0:T(8,128)(2,1)} %get-tuple-element.25.q_ref, bf16[512,512]{1,0:T(8,128)(2,1)} %get-tuple-element.26.k_ref, bf16[512,512]{1,0:T(8,128)(2,1)} %get-tuple-element.27.v_ref, bf16[2,64,512]{2,1,0:T(8,128)(2,1)} %copy-done.23, bf16[2,64,512]{2,1,0:T(8,128)(2,1)} %copy-done.25, ...), custom_call_target="tpu_custom_call" | custom-call | tf_op jit(solution)/shard_map/attention/pallas_call | solution.py:152
  124.3 2.1 collective-permute-done.14.other_ref
  126.4 0.8 copy-done.15
  127.2 3.0 %project.8 = bf16[512,512]{1,0:T(8,128)(2,1)} custom-call(s32[1]{0:T(128)} %bitcast.12.id_ref, bf16[512,512]{1,0:T(8,128)(2,1)} %attention.4.own_ref, bf16[512,512]{1,0:T(8,128)(2,1)} %copy-done.15, bf16[3,512,2048]{2,1,0:T(8,128)(2,1)} %w_own_ref.11, bf16[3,512,512]{2,1,0:T(8,128)(2,1)} %copy-done.2), custom_call_target="tpu_custom_call" | custom-call | tf_op jit(solution)/shard_map/project/pallas_call | solution.py:181
  130.3 1.6 collective-permute-start.15
  131.9 3.0 %project.9 = bf16[512,512]{1,0:T(8,128)(2,1)} custom-call(s32[1]{0:T(128)} %bitcast.17.id_ref, bf16[512,512]{1,0:T(8,128)(2,1)} %attention.4.own_ref, bf16[512,512]{1,0:T(8,128)(2,1)} %copy-done.15, bf16[3,512,2048]{2,1,0:T(8,128)(2,1)} %w_own_ref.11, bf16[3,512,512]{2,1,0:T(8,128)(2,1)} %copy-done), custom_call_target="tpu_custom_call" | custom-call | tf_op jit(solution)/shard_map/project/pallas_call | solution.py:181
  135.4 10.0 %collective-permute-done.15 = bf16[512,512]{1,0:T(8,128)(2,1)S(1)} collective-permute-done((bf16[512,512]{1,0:T(8,128)(2,1)}, bf16[512,512]{1,0:T(8,128)(2,1)S(1)}, u32[]{:S(2)}, u32[]{:S(2)}) %collective-permute-start.15) | collective-permute-done | bytes 524320 | tf_op jit(solution)/shard_map/ppermute | solution.py:280
  145.3 10.5 %collective-permute-done.16 = bf16[512,512]{1,0:T(8,128)(2,1)} collective-permute-done((bf16[512,512]{1,0:T(8,128)(2,1)}, bf16[512,512]{1,0:T(8,128)(2,1)}, u32[]{:S(2)}, u32[]{:S(2)}) %collective-permute-start.16) | collective-permute-done | bytes 524320 | tf_op jit(solution)/shard_map/ppermute | solution.py:280
  155.9 2.5 %broadcast_select_fusion.2 = (bf16[512,512]{1,0:T(8,128)(2,1)}, bf16[512,512]{1,0:T(8,128)(2,1)S(1)}, bf16[512,512]{1,0:T(8,128)(2,1)S(1)}) fusion(pred[]{:T(512)S(6)} %eq.32, bf16[512,512]{1,0:T(8,128)(2,1)} %collective-permute-done.16, bf16[512,512]{1,0:T(8,128)(2,1)} %project.9, bf16[512,512]{1,0:T(8,128)(2,1)S(1)} %copy-done.7, ...), kind=kLoop, calls=%fused_computation.27 | loop fusion | flops 3407872 | bytes 4718593 | tf_op jit(solution)/shard_map/jit(_where)/select_n | solution.py:334
  158.8 1.4 collective-permute-done.17.refs_2_
  160.2 0.9 collective-permute-done.18.refs_3_
  161.1 8.9 %qkv.5 = (bf16[512,512]{1,0:T(8,128)(2,1)}, bf16[512,512]{1,0:T(8,128)(2,1)}, bf16[512,512]{1,0:T(8,128)(2,1)}, bf16[2,64,512]{2,1,0:T(8,128)(2,1)}, bf16[2,64,512]{2,1,0:T(8,128)(2,1)}) custom-call(s32[4]{0:T(128)} %pad_add_fusion.1.ids_ref, bf16[512,512]{1,0:T(8,128)(2,1)} %copy-done.11, bf16[512,512]{1,0:T(8,128)(2,1)} %copy-done.12, ...), custom_call_target="tpu_custom_call" | custom-call | tf_op jit(solution)/shard_map/qkv/pallas_call | solution.py:89
  170.1 1.7 collective-permute-start.19
  172.2 3.7 %collective-permute-done.19.before_ref = bf16[2,64,512]{2,1,0:T(8,128)(2,1)S(1)} collective-permute-done((bf16[2,64,512]{2,1,0:T(8,128)(2,1)}, bf16[2,64,512]{2,1,0:T(8,128)(2,1)S(1)}, u32[]{:S(2)}, u32[]{:S(2)}) %collective-permute-start.19) | collective-permute-done | bytes 131104 | tf_op jit(solution)/shard_map/ppermute | solution.py:304
  175.9 1.4 collective-permute-done.20.after_ref
  177.3 0.7 copy-done.24
  177.9 5.2 %attention.5.own_ref = bf16[512,512]{1,0:T(8,128)(2,1)} custom-call(bf16[512,512]{1,0:T(8,128)(2,1)} %get-tuple-element.30.q_ref, bf16[512,512]{1,0:T(8,128)(2,1)} %get-tuple-element.31.k_ref, bf16[512,512]{1,0:T(8,128)(2,1)} %get-tuple-element.32.v_ref, bf16[2,64,512]{2,1,0:T(8,128)(2,1)} %copy-done.22, bf16[2,64,512]{2,1,0:T(8,128)(2,1)} %copy-done.24, ...), custom_call_target="tpu_custom_call" | custom-call | tf_op jit(solution)/shard_map/attention/pallas_call | solution.py:152
  183.2 1.9 broadcast_select_fusion
  185.4 3.0 %project.11 = bf16[512,512]{1,0:T(8,128)(2,1)} custom-call(s32[1]{0:T(128)} %bitcast.20.id_ref, bf16[512,512]{1,0:T(8,128)(2,1)} %attention.5.own_ref, bf16[512,512]{1,0:T(8,128)(2,1)} %collective-permute-done.21.other_ref, bf16[3,512,2048]{2,1,0:T(8,128)(2,1)} %w_own_ref.11, bf16[3,512,512]{2,1,0:T(8,128)(2,1)} %get-tuple-element.40.w_other_ref), custom_call_target="tpu_custom_call" | custom-call | tf_op jit(solution)/shard_map/project/pallas_call | solution.py:181
  188.4 1.5 collective-permute-start.22
  189.9 3.0 %project.10.refs_0_ = bf16[512,512]{1,0:T(8,128)(2,1)} custom-call(s32[1]{0:T(128)} %bitcast.13.id_ref, bf16[512,512]{1,0:T(8,128)(2,1)} %attention.5.own_ref, bf16[512,512]{1,0:T(8,128)(2,1)} %collective-permute-done.21.other_ref, bf16[3,512,2048]{2,1,0:T(8,128)(2,1)} %w_own_ref.11, bf16[3,512,512]{2,1,0:T(8,128)(2,1)} %get-tuple-element.41.w_other_ref), custom_call_target="tpu_custom_call" | custom-call | tf_op jit(solution)/shard_map/project/pallas_call | solution.py:181
  193.0 9.7 %collective-permute-done.22.refs_1_ = bf16[512,512]{1,0:T(8,128)(2,1)S(1)} collective-permute-done((bf16[512,512]{1,0:T(8,128)(2,1)}, bf16[512,512]{1,0:T(8,128)(2,1)S(1)}, u32[]{:S(2)}, u32[]{:S(2)}) %collective-permute-start.22) | collective-permute-done | bytes 524320 | tf_op jit(solution)/shard_map/ppermute | solution.py:280
  202.6 0.8 copy-done.19
  203.5 2.7 %to_row_order.1 = bf16[512,512]{1,0:T(8,128)(2,1)} custom-call(bf16[512,512]{1,0:T(8,128)(2,1)} %get-tuple-element.35.x_ref, bf16[512,512]{1,0:T(8,128)(2,1)} %project.10.refs_0_, bf16[512,512]{1,0:T(8,128)(2,1)} %copy-done.19), custom_call_target="tpu_custom_call" | custom-call | tf_op jit(solution)/shard_map/to_row_order/pallas_call | solution.py:215
  206.2 17.9 %all_to_all.10 = bf16[8,64,512]{2,1,0:T(8,128)(2,1)S(1)} all-to-all(bf16[8,64,512]{2,1,0:T(8,128)(2,1)} %bitcast.68), channel_id=1, replica_groups=mesh['sp'=8,'tp'=4] {'sp'}, dimensions={0} | all-to-all | bytes 1048576 | tf_op jit(solution)/shard_map/all_to_all | solution.py:344
  224.2 1.0 copy.13
  (94 shorter events, 7.3 us)
Async XLA Ops:
  6.3 21.9 %all-to-all-start = ((bf16[8,64,512]{2,1,0:T(8,128)(2,1)}), bf16[8,64,512]{2,1,0:T(8,128)(2,1)}, u32[]{:S(2)}, u32[]{:S(2)}) async-start(bf16[8,64,512]{2,1,0:T(8,128)(2,1)} %fusion.24), calls=%async_computation | async-start | bytes 1048576 | tf_op jit(solution)/shard_map/all_to_all | solution.py:284
  13.6 4.6 %copy-start.27 = (bf16[3,2048]{1,0:T(4,128)(2,1)S(1)}, bf16[3,2048]{1,0:T(4,128)(2,1)}, u32[]{:S(2)}) copy-start(bf16[3,2048]{1,0:T(4,128)(2,1)} %param.8) | copy-start | bytes 36868
  13.6 5.2 %copy-start.26 = (f32[3,8,8,16]{3,2,1,0:T(8,128)S(1)}, f32[3,8,8,16]{3,2,1,0:T(8,128)}, u32[]{:S(2)}) copy-start(f32[3,8,8,16]{3,2,1,0:T(8,128)} %param.13) | copy-start | bytes 36868
  17.7 49.0 %collective-permute-start.8 = (bf16[3,512,512]{2,1,0:T(8,128)(2,1)}, bf16[3,512,512]{2,1,0:T(8,128)(2,1)S(1)}, u32[]{:S(2)}, u32[]{:S(2)}) collective-permute-start(bf16[3,512,512]{2,1,0:T(8,128)(2,1)} %get-tuple-element.39), channel_id=1, source_target_pairs={{0,1},{1,0},{2,3},{3,2},{4,5},{5,4},{6,7},{7,6},{8,9},{9,8},{10,11... | collective-permute-start | bytes 4718600 | tf_op jit(solution)/shard_map/ppermute | solution.py:277
  17.7 55.8 %collective-permute-start.6 = (bf16[3,512,512]{2,1,0:T(8,128)(2,1)}, bf16[3,512,512]{2,1,0:T(8,128)(2,1)S(1)}, u32[]{:S(2)}, u32[]{:S(2)}) collective-permute-start(bf16[3,512,512]{2,1,0:T(8,128)(2,1)} %get-tuple-element.38), channel_id=1, source_target_pairs={{0,1},{1,0},{2,3},{3,2},{4,5},{5,4},{6,7},{7,6},{8,9},{9,8},{10,11... | collective-permute-start | bytes 4718600 | tf_op jit(solution)/shard_map/ppermute | solution.py:277
  30.5 12.5 %collective-permute-start = (bf16[512,512]{1,0:T(8,128)(2,1)}, bf16[512,512]{1,0:T(8,128)(2,1)S(1)}, u32[]{:S(2)}, u32[]{:S(2)}) collective-permute-start(bf16[512,512]{1,0:T(8,128)(2,1)} %to_column_order.1.refs_0_), channel_id=1, source_target_pairs={{0,2},{1,3},{2,0},{3,1},{4,6},{5,7},{6,4},{7,5},{8,10},{9,11},{10,... | collective-permute-start | bytes 1572872 | tf_op jit(solution)/shard_map/ppermute | solution.py:280
  32.0 12.5 %collective-permute-start.1 = (bf16[512,512]{1,0:T(8,128)(2,1)}, bf16[512,512]{1,0:T(8,128)(2,1)}, u32[]{:S(2)}, u32[]{:S(2)}) collective-permute-start(bf16[512,512]{1,0:T(8,128)(2,1)} %to_column_order.1.refs_0_), channel_id=1, source_target_pairs={{0,1},{1,0},{2,3},{3,2},{4,5},{5,4},{6,7},{7,6},{8,9},{9,8},{10,11... | collective-permute-start | bytes 1572872 | tf_op jit(solution)/shard_map/ppermute | solution.py:277
  43.0 0.8 copy-start.9
  43.8 2.0 collective-permute-start.2
  54.6 6.1 %collective-permute-start.3 = (bf16[2,64,512]{2,1,0:T(8,128)(2,1)}, bf16[2,64,512]{2,1,0:T(8,128)(2,1)S(1)}, u32[]{:S(2)}, u32[]{:S(2)}) collective-permute-start(bf16[2,64,512]{2,1,0:T(8,128)(2,1)} %get-tuple-element.23), channel_id=1, source_target_pairs={{0,8},{8,16},{16,24},{24,28},{28,20},{20,12},{12,4},{4,0},{1,9},{9... | collective-permute-start | bytes 393224 | tf_op jit(solution)/shard_map/ppermute | solution.py:304
  54.6 6.1 %collective-permute-start.4 = (bf16[2,64,512]{2,1,0:T(8,128)(2,1)}, bf16[2,64,512]{2,1,0:T(8,128)(2,1)S(1)}, u32[]{:S(2)}, u32[]{:S(2)}) collective-permute-start(bf16[2,64,512]{2,1,0:T(8,128)(2,1)} %get-tuple-element.24), channel_id=1, source_target_pairs={{8,0},{16,8},{24,16},{28,24},{20,28},{12,20},{4,12},{0,4},{9,1},{1... | collective-permute-start | bytes 393224 | tf_op jit(solution)/shard_map/ppermute | solution.py:303
  60.7 0.7 copy-start.20
  60.7 0.7 copy-start.21
  66.6 2.3 %collective-permute-start.5 = (bf16[512,512]{1,0:T(8,128)(2,1)}, bf16[512,512]{1,0:T(8,128)(2,1)}, u32[]{:S(2)}, u32[]{:S(2)}) collective-permute-start(bf16[512,512]{1,0:T(8,128)(2,1)} %attention.3.own_ref), channel_id=1, source_target_pairs={{0,1},{1,0},{2,3},{3,2},{4,5},{5,4},{6,7},{7,6},{8,9},{9,8},{10,11... | collective-permute-start | bytes 1572872 | tf_op jit(solution)/shard_map/ppermute | solution.py:277
  66.6 2.2 copy-start
  72.0 15.1 %collective-permute-start.9 = (bf16[512,512]{1,0:T(8,128)(2,1)}, bf16[512,512]{1,0:T(8,128)(2,1)}, u32[]{:S(2)}, u32[]{:S(2)}) collective-permute-start(bf16[512,512]{1,0:T(8,128)(2,1)} %project.7), channel_id=1, source_target_pairs={{0,2},{1,3},{2,0},{3,1},{4,6},{5,7},{6,4},{7,5},{8,10},{9,11},{10,... | collective-permute-start | bytes 1572872 | tf_op jit(solution)/shard_map/ppermute | solution.py:280
  73.5 1.1 copy-start.2
  74.6 22.7 %copy-start.8 = (bf16[512,512]{1,0:T(8,128)(2,1)S(1)}, bf16[512,512]{1,0:T(8,128)(2,1)}, u32[]{:S(2)}) copy-start(bf16[512,512]{1,0:T(8,128)(2,1)} %to_column_order.1.refs_0_) | copy-start | bytes 1572868
  74.6 22.7 %copy-start.10 = (bf16[512,512]{1,0:T(8,128)(2,1)S(1)}, bf16[512,512]{1,0:T(8,128)(2,1)}, u32[]{:S(2)}) copy-start(bf16[512,512]{1,0:T(8,128)(2,1)} %copy-done.9) | copy-start | bytes 1572868
  74.6 22.7 %copy-start.13 = (bf16[512,512]{1,0:T(8,128)(2,1)S(1)}, bf16[512,512]{1,0:T(8,128)(2,1)}, u32[]{:S(2)}) copy-start(bf16[512,512]{1,0:T(8,128)(2,1)} %project.7) | copy-start | bytes 1572868
  77.8 19.6 %collective-permute-start.7 = (bf16[512,512]{1,0:T(8,128)(2,1)}, bf16[512,512]{1,0:T(8,128)(2,1)S(1)}, u32[]{:S(2)}, u32[]{:S(2)}) collective-permute-start(bf16[512,512]{1,0:T(8,128)(2,1)} %project.6), channel_id=1, source_target_pairs={{0,2},{1,3},{2,0},{3,1},{4,6},{5,7},{6,4},{7,5},{8,10},{9,11},{10,... | collective-permute-start | bytes 1572872 | tf_op jit(solution)/shard_map/ppermute | solution.py:280
  99.0 2.8 %copy-start.4 = (bf16[512,512]{1,0:T(8,128)(2,1)}, bf16[512,512]{1,0:T(8,128)(2,1)S(1)}, u32[]{:S(2)}) copy-start(bf16[512,512]{1,0:T(8,128)(2,1)S(1)} %get-tuple-element.42.refs_1_) | copy-start | bytes 1572868
  99.0 2.7 %copy-start.6 = (bf16[512,512]{1,0:T(8,128)(2,1)}, bf16[512,512]{1,0:T(8,128)(2,1)S(1)}, u32[]{:S(2)}) copy-start(bf16[512,512]{1,0:T(8,128)(2,1)S(1)} %get-tuple-element.43.refs_0_) | copy-start | bytes 1572868
  99.1 2.0 collective-permute-start.10
  99.1 2.6 %collective-permute-start.11 = (bf16[512,512]{1,0:T(8,128)(2,1)S(1)}, bf16[512,512]{1,0:T(8,128)(2,1)S(1)}, u32[]{:S(2)}, u32[]{:S(2)}) collective-permute-start(bf16[512,512]{1,0:T(8,128)(2,1)S(1)} %get-tuple-element.42.refs_1_), channel_id=1, source_target_pairs={{0,1},{1,0},{2,3},{3,2},{4,5},{5,4},{6,7},{7,6},{8,9},{9,8},{10,11... | collective-permute-start | bytes 1572872 | tf_op jit(solution)/shard_map/ppermute | solution.py:277
  101.0 0.8 copy-start.16
  101.8 0.8 copy-start.18
  111.5 5.8 %collective-permute-start.12 = (bf16[2,64,512]{2,1,0:T(8,128)(2,1)}, bf16[2,64,512]{2,1,0:T(8,128)(2,1)S(1)}, u32[]{:S(2)}, u32[]{:S(2)}) collective-permute-start(bf16[2,64,512]{2,1,0:T(8,128)(2,1)} %get-tuple-element.28), channel_id=1, source_target_pairs={{0,8},{8,16},{16,24},{24,28},{28,20},{20,12},{12,4},{4,0},{1,9},{9... | collective-permute-start | bytes 393224 | tf_op jit(solution)/shard_map/ppermute | solution.py:304
  113.0 5.5 %collective-permute-start.13 = (bf16[2,64,512]{2,1,0:T(8,128)(2,1)}, bf16[2,64,512]{2,1,0:T(8,128)(2,1)S(1)}, u32[]{:S(2)}, u32[]{:S(2)}) collective-permute-start(bf16[2,64,512]{2,1,0:T(8,128)(2,1)} %get-tuple-element.29), channel_id=1, source_target_pairs={{8,0},{16,8},{24,16},{28,24},{20,28},{12,20},{4,12},{0,4},{9,1},{1... | collective-permute-start | bytes 393224 | tf_op jit(solution)/shard_map/ppermute | solution.py:303
  117.3 1.2 copy-start.23
  118.4 0.7 copy-start.25
  124.3 2.1 collective-permute-start.14
  126.4 0.8 copy-start.15
  130.3 25.6 %copy-start.5 = (bf16[512,512]{1,0:T(8,128)(2,1)S(1)}, bf16[512,512]{1,0:T(8,128)(2,1)}, u32[]{:S(2)}) copy-start(bf16[512,512]{1,0:T(8,128)(2,1)} %copy-done.4) | copy-start | bytes 1572868
  130.3 25.6 %copy-start.7 = (bf16[512,512]{1,0:T(8,128)(2,1)S(1)}, bf16[512,512]{1,0:T(8,128)(2,1)}, u32[]{:S(2)}) copy-start(bf16[512,512]{1,0:T(8,128)(2,1)} %copy-done.6) | copy-start | bytes 1572868
  130.3 25.6 %copy-start.14 = (bf16[512,512]{1,0:T(8,128)(2,1)S(1)}, bf16[512,512]{1,0:T(8,128)(2,1)}, u32[]{:S(2)}) copy-start(bf16[512,512]{1,0:T(8,128)(2,1)} %project.8) | copy-start | bytes 1572868
  130.3 15.1 %collective-permute-start.15 = (bf16[512,512]{1,0:T(8,128)(2,1)}, bf16[512,512]{1,0:T(8,128)(2,1)S(1)}, u32[]{:S(2)}, u32[]{:S(2)}) collective-permute-start(bf16[512,512]{1,0:T(8,128)(2,1)} %project.8), channel_id=1, source_target_pairs={{0,2},{1,3},{2,0},{3,1},{4,6},{5,7},{6,4},{7,5},{8,10},{9,11},{10,... | collective-permute-start | bytes 1572872 | tf_op jit(solution)/shard_map/ppermute | solution.py:280
  134.9 21.0 %collective-permute-start.16 = (bf16[512,512]{1,0:T(8,128)(2,1)}, bf16[512,512]{1,0:T(8,128)(2,1)}, u32[]{:S(2)}, u32[]{:S(2)}) collective-permute-start(bf16[512,512]{1,0:T(8,128)(2,1)} %project.9), channel_id=1, source_target_pairs={{0,2},{1,3},{2,0},{3,1},{4,6},{5,7},{6,4},{7,5},{8,10},{9,11},{10,... | collective-permute-start | bytes 1572872 | tf_op jit(solution)/shard_map/ppermute | solution.py:280
  158.3 2.8 %copy-start.11 = (bf16[512,512]{1,0:T(8,128)(2,1)}, bf16[512,512]{1,0:T(8,128)(2,1)S(1)}, u32[]{:S(2)}) copy-start(bf16[512,512]{1,0:T(8,128)(2,1)S(1)} %get-tuple-element.36.refs_0_) | copy-start | bytes 1572868
  158.3 2.8 %copy-start.12 = (bf16[512,512]{1,0:T(8,128)(2,1)}, bf16[512,512]{1,0:T(8,128)(2,1)S(1)}, u32[]{:S(2)}) copy-start(bf16[512,512]{1,0:T(8,128)(2,1)S(1)} %get-tuple-element.37.refs_1_) | copy-start | bytes 1572868
  158.3 1.9 collective-permute-start.17
  158.3 2.8 %collective-permute-start.18 = (bf16[512,512]{1,0:T(8,128)(2,1)S(1)}, bf16[512,512]{1,0:T(8,128)(2,1)}, u32[]{:S(2)}, u32[]{:S(2)}) collective-permute-start(bf16[512,512]{1,0:T(8,128)(2,1)S(1)} %get-tuple-element.37.refs_1_), channel_id=1, source_target_pairs={{0,1},{1,0},{2,3},{3,2},{4,5},{5,4},{6,7},{7,6},{8,9},{9,8},{10,11... | collective-permute-start | bytes 1572872 | tf_op jit(solution)/shard_map/ppermute | solution.py:277
  160.2 0.9 copy-start.17
  161.1 22.0 %copy-start.3 = (bf16[3,512,512]{2,1,0:T(8,128)(2,1)S(1)}, bf16[3,512,512]{2,1,0:T(8,128)(2,1)}, u32[]{:S(2)}) copy-start(bf16[3,512,512]{2,1,0:T(8,128)(2,1)} %copy-done.2) | copy-start | bytes 4718596
  170.1 13.1 %copy-start.1 = (bf16[3,512,512]{2,1,0:T(8,128)(2,1)S(1)}, bf16[3,512,512]{2,1,0:T(8,128)(2,1)}, u32[]{:S(2)}) copy-start(bf16[3,512,512]{2,1,0:T(8,128)(2,1)} %copy-done) | copy-start | bytes 4718596
  170.1 5.8 %collective-permute-start.19 = (bf16[2,64,512]{2,1,0:T(8,128)(2,1)}, bf16[2,64,512]{2,1,0:T(8,128)(2,1)S(1)}, u32[]{:S(2)}, u32[]{:S(2)}) collective-permute-start(bf16[2,64,512]{2,1,0:T(8,128)(2,1)} %get-tuple-element.33), channel_id=1, source_target_pairs={{0,8},{8,16},{16,24},{24,28},{28,20},{20,12},{12,4},{4,0},{1,9},{9... | collective-permute-start | bytes 393224 | tf_op jit(solution)/shard_map/ppermute | solution.py:304
  171.8 5.5 %collective-permute-start.20 = (bf16[2,64,512]{2,1,0:T(8,128)(2,1)}, bf16[2,64,512]{2,1,0:T(8,128)(2,1)S(1)}, u32[]{:S(2)}, u32[]{:S(2)}) collective-permute-start(bf16[2,64,512]{2,1,0:T(8,128)(2,1)} %get-tuple-element.34), channel_id=1, source_target_pairs={{8,0},{16,8},{24,16},{28,24},{20,28},{12,20},{4,12},{0,4},{9,1},{1... | collective-permute-start | bytes 393224 | tf_op jit(solution)/shard_map/ppermute | solution.py:303
  175.9 1.4 copy-start.22
  177.3 0.7 copy-start.24
  183.1 2.3 %collective-permute-start.21 = (bf16[512,512]{1,0:T(8,128)(2,1)}, bf16[512,512]{1,0:T(8,128)(2,1)}, u32[]{:S(2)}, u32[]{:S(2)}) collective-permute-start(bf16[512,512]{1,0:T(8,128)(2,1)} %attention.5.own_ref), channel_id=1, source_target_pairs={{0,1},{1,0},{2,3},{3,2},{4,5},{5,4},{6,7},{7,6},{8,9},{9,8},{10,11... | collective-permute-start | bytes 1572872 | tf_op jit(solution)/shard_map/ppermute | solution.py:277
  188.4 14.2 %collective-permute-start.22 = (bf16[512,512]{1,0:T(8,128)(2,1)}, bf16[512,512]{1,0:T(8,128)(2,1)S(1)}, u32[]{:S(2)}, u32[]{:S(2)}) collective-permute-start(bf16[512,512]{1,0:T(8,128)(2,1)} %project.11), channel_id=1, source_target_pairs={{0,2},{1,3},{2,0},{3,1},{4,6},{5,7},{6,4},{7,5},{8,10},{9,11},{10,... | collective-permute-start | bytes 1572872 | tf_op jit(solution)/shard_map/ppermute | solution.py:280
  202.6 0.8 copy-start.19

commit v2 on v0

v2 whole, which is shorter than its diff:
```python
import functools
import math

import jax
import jax.numpy as jnp
from jax import lax
from jax.experimental import pallas as pl
from jax.experimental.pallas import tpu as pltpu
from jax.sharding import PartitionSpec as P

HEAD_DIM = 64
WIN_R = 8
WIN_C = 16
HALF_R = WIN_R // 2
HALF_C = WIN_C // 2
EPS = 1e-06
LOG2E = math.log2(math.e)
Q_SCALE = HEAD_DIM ** (-0.5) * LOG2E
MASKED = -1e30
BLOCK = 128
F32 = jnp.float32
BF16 = jnp.bfloat16
VMEM_LIMIT = 14 * 1024 * 1024
NT = (((1,), (1,)), ((), ()))
TN = (((0,), (0,)), ((), ()))


def call(kernel, name, outs, *args, scalars=(), scratch=()):
    vmem = pl.BlockSpec(memory_space=pltpu.VMEM)
    smem = pl.BlockSpec(memory_space=pltpu.SMEM)
    return pl.pallas_call(
        kernel,
        in_specs=[smem] * len(scalars) + [vmem] * len(args),
        out_specs=[vmem] * len(outs),
        out_shape=[jax.ShapeDtypeStruct(shape, dtype) for shape, dtype in outs],
        scratch_shapes=list(scratch),
        compiler_params=pltpu.CompilerParams(vmem_limit_bytes=VMEM_LIMIT),
        name=name,
    )(*scalars, *args)


def one_hot(pick):
    return pick.astype(F32).astype(BF16)


def split_columns(x, picks, n_sp):
    chunk, columns = x.shape

    def kernel(x_ref, *outs):
        for out, (cols_of, rank) in zip(outs, picks):
            width = len(cols_of)
            at = lax.broadcasted_iota(jnp.int32, (width, columns), 0)
            source = lax.broadcasted_iota(jnp.int32, (width, columns), 1)
            local = part_column(at, cols_of)
            for device in range(n_sp):
                first = rank[device] * (columns // n_sp)
                out[device] = lax.dot_general(
                    one_hot(source == local + first), x_ref[...], NT, preferred_element_type=F32
                ).astype(BF16)

    outs = [((n_sp, len(cols_of), chunk), BF16) for cols_of, _ in picks]
    return call(kernel, "split_columns", outs, x)


def part_column(at, cols_of):
    jump = next((i for i in range(1, len(cols_of)) if cols_of[i] != cols_of[i - 1] + 1), None)
    local = at + cols_of[0]
    if jump is not None:
        local = local + jnp.where(at >= jump, cols_of[jump] - cols_of[0] - jump, 0)
    return local


def merge_columns(parts, picks, columns, n_sp):
    chunk = parts[0].shape[2]
    per = columns // n_sp

    def kernel(*refs):
        out = refs[-1]
        acc = jnp.zeros((chunk, columns), F32)
        for ref, (cols_of, rank) in zip(refs, picks):
            width = len(cols_of)
            at = lax.broadcasted_iota(jnp.int32, (width, columns), 0)
            target = lax.broadcasted_iota(jnp.int32, (width, columns), 1)
            local = part_column(at, cols_of)
            pick = jnp.concatenate(
                [one_hot(target == local + rank[device] * per) for device in range(n_sp)], axis=0
            )
            rows = jnp.concatenate([ref[device] for device in range(n_sp)], axis=0)
            acc = acc + lax.dot_general(rows, pick, TN, preferred_element_type=F32)
        out[...] = acc.astype(BF16)

    return call(kernel, "merge_columns", [((chunk, columns), BF16)], *parts)[0]


def to_column_order(x):
    rows, cols, chunk = x.shape
    tokens = rows * cols

    def kernel(x_ref, o_ref):
        out_at = lax.broadcasted_iota(jnp.int32, (tokens, tokens), 0)
        in_at = lax.broadcasted_iota(jnp.int32, (tokens, tokens), 1)
        pick = one_hot((out_at % rows) * cols + out_at // rows == in_at)
        source = jnp.concatenate([x_ref[row] for row in range(rows)], axis=0)
        o_ref[...] = jnp.dot(pick, source, preferred_element_type=F32).astype(BF16)

    return call(kernel, "to_column_order", [((tokens, chunk), BF16)], x)[0]


def expand_bias(bases, rows):
    tables, _, window = bases.shape

    def kernel(base_ref, o_ref):
        def one(table, carry):
            base = base_ref[table]
            for col in range(BLOCK // rows):
                shifted = base if col == 0 else pltpu.roll(base, col * rows, 1)
                o_ref[table, col * rows : (col + 1) * rows] = shifted
            return carry

        lax.fori_loop(0, tables, one, 0)

    return call(kernel, "expand_bias", [((tables, BLOCK, window), F32)], bases)[0]


def qkv(layer, parts, ids, gains, w_query, w_key, w_value, halo):
    tokens = parts[0].shape[0]
    chunk = gains.shape[3]
    n_tp = gains.shape[1]
    d_model = n_tp * chunk
    channels = w_query.shape[2]
    pieces = [(i, lo) for i, part in enumerate(parts) for lo in range(0, part.shape[1], chunk)]

    def kernel(ids_ref, *refs):
        ins = refs[: len(parts)]
        gain_ref, wq_ref, wk_ref, wv_ref = refs[len(parts) : len(parts) + 4]
        outs = refs[len(parts) + 4 : -1]
        scaled_ref = refs[-1]
        squares = jnp.zeros((tokens, 128), F32)
        for at, (i, lo) in enumerate(pieces):
            wide = ins[i][:, lo : lo + chunk].astype(F32)
            where = ids_ref[at]
            scaled_ref[where] = (wide * gain_ref[layer, where]).astype(BF16)
            for lane in range(0, chunk, 128):
                tile = wide[:, lane : lane + 128]
                squares = squares + tile * tile
        inverse = lax.rsqrt(jnp.sum(squares, axis=1, keepdims=True) / d_model + EPS)
        scaled = jnp.concatenate([scaled_ref[at] for at in range(n_tp)], axis=1)

        def times(w_ref, scale):
            return (jnp.dot(scaled, w_ref[layer], preferred_element_type=F32) * scale).astype(BF16)

        for at, w_ref in ((1, wk_ref), (2, wv_ref)):
            out = times(w_ref, inverse)
            outs[at][...] = out
            if halo:
                outs[3][at - 1] = out[:halo]
                outs[4][at - 1] = out[tokens - halo :]
        outs[0][...] = times(wq_ref, inverse * Q_SCALE)

    outs = [((tokens, channels), BF16)] * 3
    if halo:
        outs += [((2, halo, channels), BF16)] * 2
    return call(
        kernel,
        "qkv",
        outs,
        *parts,
        gains,
        w_query,
        w_key,
        w_value,
        scalars=(ids,),
        scratch=[pltpu.VMEM((n_tp, tokens, chunk), BF16)],
    )


def attention(layer, starts, q, sources, segments, bias):
    tokens, channels = q.shape
    window = bias.shape[2]
    halo = (window - BLOCK) // 2
    width = 2 * HEAD_DIM
    heads = channels // HEAD_DIM

    def kernel(q_ref, *refs):
        bias_ref, o_ref = refs[-2:]

        def read(of_value, low, lanes):
            pieces = []
            for first, rows, source, row in segments:
                lo, hi = max(low, first), min(low + window, first + rows)
                if lo >= hi:
                    continue
                at = slice(row + lo - first, row + hi - first)
                if isinstance(source, tuple):
                    pieces.append(refs[source[of_value]][at, lanes])
                else:
                    pieces.append(refs[source][of_value, at, lanes])
            return jnp.concatenate(pieces, axis=0)

        low_half = lax.broadcasted_iota(jnp.int32, (BLOCK, width), 1) < HEAD_DIM
        ones = jnp.ones((window, width), BF16)

        def one_pair(pair, carry):
            lanes = pl.ds(pl.multiple_of(pair * width, width), width)
            for at, start in enumerate(starts):
                rows = slice(at * BLOCK, (at + 1) * BLOCK)
                q_wide = q_ref[rows, lanes].astype(F32)
                both = jnp.concatenate(
                    [jnp.where(low_half, q_wide, 0.0), jnp.where(low_half, 0.0, q_wide)], axis=0
                )
                scores = lax.dot_general(
                    both.astype(BF16),
                    read(0, start - halo, lanes),
                    NT,
                    preferred_element_type=F32,
                )
                table = layer * heads + 2 * pair
                scores = scores + jnp.concatenate([bias_ref[table], bias_ref[table + 1]], axis=0)
                highest = jnp.max(scores, axis=1, keepdims=True)
                weights = jnp.exp2(scores - highest).astype(BF16)
                values = jnp.concatenate([read(1, start - halo, lanes), ones], axis=1)
                mixed = jnp.dot(weights, values, preferred_element_type=F32)
                top = jnp.where(low_half, mixed[:BLOCK, :width], mixed[BLOCK:, :width])
                total = jnp.where(low_half, mixed[:BLOCK, width:], mixed[BLOCK:, width:])
                o_ref[rows, lanes] = (top / total).astype(BF16)
            return carry

        lax.fori_loop(0, channels // width, one_pair, 0)

    return call(kernel, "attention", [((tokens, channels), BF16)], q, *sources, bias)[0]


def project(layer, own, other, w_out, w_other, ys, my_core, joined):
    tokens, channels = own.shape
    chunk = w_other.shape[3]
    count = ys.shape[0]

    def kernel(ys_ref, core_ref, own_ref, other_ref, w_out_ref, w_other_ref, *outs):
        for at in range(count):
            y = ys_ref[at]
            column = pl.multiple_of((2 * y + core_ref[0]) * chunk, chunk)
            acc = jnp.dot(
                own_ref[...], w_out_ref[layer, :, pl.ds(column, chunk)], preferred_element_type=F32
            )
            acc = acc + jnp.dot(other_ref[...], w_other_ref[y, layer], preferred_element_type=F32)
            if joined:
                outs[0][:, at * chunk : (at + 1) * chunk] = acc.astype(BF16)
            else:
                outs[at][...] = acc.astype(BF16)

    if joined:
        outs = [((tokens, count * chunk), BF16)]
    else:
        outs = [((tokens, chunk), BF16)] * count
    return call(
        kernel, "project", outs, own, other, w_out, w_other, scalars=(ys, my_core.reshape(1))
    )


def add_update(olds, partials, orders):
    tokens, wide = partials[0].shape
    chunk = wide // (wide // olds[0].shape[1]) if len(olds) > 1 else wide

    def kernel(where_ref, *refs):
        old_refs, partial_refs, o_ref = refs[: len(olds)], refs[len(olds) : -1], refs[-1]
        for at, lo in enumerate(range(0, wide, chunk)):
            old = old_refs[0][...].astype(F32)
            for piece in range(1, len(olds)):
                fresh = old_refs[piece][...].astype(F32)
                old = jnp.where(where_ref[at] == piece, fresh, old)
            update = partial_refs[0][:, lo : lo + chunk].astype(F32)
            for ref in partial_refs[1:]:
                update = update + ref[:, lo : lo + chunk].astype(F32)
            o_ref[:, lo : lo + chunk] = (old + update).astype(BF16)

    return call(
        kernel, "add_update", [((tokens, wide), BF16)], *olds, *partials, scalars=(orders,)
    )[0]


def finish(old, partials, my_y, rows, cols):
    tokens, chunk = partials[0].shape

    def kernel(y_ref, old_ref, *refs):
        o_ref = refs[-1]
        grid = old_ref[:, :chunk].astype(F32)
        for y in range(1, old.shape[1] // chunk):
            grid = jnp.where(y_ref[0] == y, old_ref[:, y * chunk : (y + 1) * chunk].astype(F32), grid)
        update = refs[0][...].astype(F32)
        for ref in refs[1:-1]:
            update = update + ref[...].astype(F32)
        grid = (grid + update).astype(BF16)
        out_at = lax.broadcasted_iota(jnp.int32, (tokens, tokens), 0)
        in_at = lax.broadcasted_iota(jnp.int32, (tokens, tokens), 1)
        pick = one_hot((out_at % cols) * rows + out_at // cols == in_at)
        moved = jnp.dot(pick, grid, preferred_element_type=F32).astype(BF16)
        for row in range(rows):
            o_ref[row] = moved[row * cols : (row + 1) * cols]

    return call(
        kernel, "finish", [((rows, cols, chunk), BF16)], old, *partials, scalars=(my_y.reshape(1),)
    )[0]


def ring_order(mesh):
    n_sp = mesh.shape["sp"]
    at = list(mesh.axis_names).index("sp")
    devices = mesh.devices if at == 0 else mesh.devices.T
    try:
        places = [tuple(devices[i].flat[0].coords) for i in range(n_sp)]
    except Exception:
        return list(range(n_sp))
    xs = sorted({p[0] for p in places})
    zs = sorted({p[2] for p in places})
    index = {(p[0], p[2]): i for i, p in enumerate(places)}
    if len(index) != n_sp or len(xs) * len(zs) != n_sp:
        return list(range(n_sp))
    path = [(xs[0], z) for z in zs]
    for turn, z in enumerate(reversed(zs)):
        line = xs[1:] if turn % 2 == 0 else xs[1:][::-1]
        path += [(x, z) for x in line]
    return [index[p] for p in path]


def dense_bias(rel_bias, rows, window):
    layers, heads = rel_bias.shape[:2]
    span = WIN_C * rows
    slot = lax.broadcasted_iota(jnp.int32, (WIN_R * WIN_C, rows * span), 0)
    place = lax.broadcasted_iota(jnp.int32, (WIN_R * WIN_C, rows * span), 1)
    row_slot = (place % rows - place // span + HALF_R) % rows
    col_slot = (place % span) // rows
    pick = (slot // WIN_C == row_slot) & (slot % WIN_C == col_slot)
    flat = rel_bias.reshape(layers * heads, WIN_R * WIN_C) * LOG2E
    base = jnp.dot(flat, pick.astype(F32), precision=lax.Precision.HIGHEST)
    base = jnp.where(row_slot[:1] < WIN_R, base, MASKED)
    base = base.reshape(layers * heads, rows, span)
    return jnp.pad(base, ((0, 0), (0, 0), (0, window - span)), constant_values=MASKED)


def body(token_grid, norm_gain, w_query, w_key, w_value, w_out, rel_bias, *, order):
    n_sp = lax.axis_size("sp")
    n_tp = lax.axis_size("tp")
    n_y = n_tp // 2
    layers = norm_gain.shape[0]
    chunk = token_grid.shape[1]
    columns = token_grid.shape[2]
    rows = n_sp * token_grid.shape[0]
    cols = columns // n_sp
    tokens = rows * cols
    halo = HALF_C * rows
    window = BLOCK + 2 * halo
    here = lax.axis_index("tp").astype(jnp.int32)
    my_y, my_core = here // 2, here % 2
    rank = [order.index(i) for i in range(n_sp)]
    after_of = [(order[i], order[(i + 1) % n_sp]) for i in range(n_sp)]
    before_of = [(b, a) for a, b in after_of]

    if tokens == 4 * BLOCK and halo <= BLOCK and BLOCK % rows == 0:
        per = BLOCK // rows
        parts = [
            (list(range(per, 3 * per)), [BLOCK, 2 * BLOCK]),
            (list(range(per)) + list(range(3 * per, 4 * per)), [0, 3 * BLOCK]),
        ]
    else:
        parts = [(list(range(cols)), list(range(0, tokens, BLOCK)))]
    count = len(parts)

    def over_core(x):
        return lax.ppermute(x, "tp", [(i, i ^ 1) for i in range(n_tp)])

    def over_y(x, shift):
        return lax.ppermute(x, "tp", [(i, (i + 2 * shift) % n_tp) for i in range(n_tp)])

    picks = [(cols_of, rank) for cols_of, _ in parts]
    sends = split_columns(token_grid[0], picks, n_sp)
    mine = []
    for send in sends:
        got = lax.all_to_all(send, "sp", 0, 0, tiled=True)
        mine.append(to_column_order(got))

    theirs = [
        lax.dynamic_slice_in_dim(w_out, (2 * y + 1 - my_core) * chunk, chunk, 2)
        for y in range(n_y)
    ]
    w_other = over_core(jnp.stack(theirs))
    gains = norm_gain.astype(F32).reshape(layers, n_tp, 1, chunk)
    bias = expand_bias(dense_bias(rel_bias, rows, window), rows)

    behind = [(my_y - shift) % n_y for shift in range(n_y)]
    ahead = [(my_y + shift) % n_y for shift in range(n_y)]
    every = [jnp.int32(y) for y in range(n_y)]

    def chunk_ids(ys):
        return jnp.stack([2 * y + my_core for y in ys] + [2 * y + 1 - my_core for y in ys])

    grids = [[x] + [over_y(x, shift) for shift in range(1, n_y)] for x in mine]
    for layer in range(layers):
        ids = chunk_ids(behind if layer == 0 else every)
        made = []
        for at, grid in enumerate(grids):
            made.append(
                qkv(
                    layer,
                    grid + [over_core(x) for x in grid],
                    ids,
                    gains,
                    w_query,
                    w_key,
                    w_value,
                    halo if at == count - 1 else 0,
                )
            )
        first, last = made[-1][3:]
        after = lax.ppermute(first, "sp", before_of)
        before = lax.ppermute(last, "sp", after_of)
        own_kv = [array for one in made for array in one[1:3]]
        segments = []
        for at, (_, starts) in enumerate(parts):
            for i, start in enumerate(starts):
                segments.append((start, BLOCK, (2 * at, 2 * at + 1), i * BLOCK))
        ends = [
            (-halo, halo, 2 * count, 0),
            (tokens, halo, 2 * count + 1, 0),
        ]
        fresh = []
        for at, (cols_of, starts) in enumerate(parts):
            last_part = at == count - 1
            mixed = attention(
                layer,
                starts,
                made[at][0],
                own_kv + ([before, after] if last_part else []),
                sorted(segments + (ends if last_part else [])),
                bias,
            )
            mixed_other = over_core(mixed)
            if layer + 1 < layers:
                partial = project(
                    layer, mixed, mixed_other, w_out, w_other, jnp.stack(every), my_core, True
                )[0]
                partials = [partial] + [over_y(partial, shift) for shift in range(1, n_y)]
                if layer == 0:
                    where = jnp.stack([(my_y - y) % n_y for y in every])
                else:
                    where = jnp.zeros((n_y,), jnp.int32)
                fresh.append([add_update(grids[at], partials, where)])
            else:
                ys = jnp.stack(ahead[1:] + ahead[:1])
                made_of = project(layer, mixed, mixed_other, w_out, w_other, ys, my_core, False)
                partials = [made_of[-1]]
                partials += [over_y(made_of[shift - 1], shift) for shift in range(1, n_y)]
                done = finish(grids[at][0], partials, my_y, rows, len(cols_of))
                fresh.append(lax.all_to_all(done, "sp", 0, 0, tiled=True))
        grids = fresh

    return merge_columns(grids, picks, columns, n_sp)[None]


def solution(mesh):
    in_specs = (
        P("sp", "tp", None),
        P(),
        P(None, None, "tp"),
        P(None, None, "tp"),
        P(None, None, "tp"),
        P(None, "tp", None),
        P(None, "tp", None, None),
    )
    out_specs = P("sp", "tp", None)
    return jax.shard_map(
        functools.partial(body, order=ring_order(mesh)),
        mesh=mesh,
        in_specs=in_specs,
        out_specs=out_specs,
        check_vma=False,
    )
```

time: 1070 us -> 212 us (0.20)
  waiting for transfers between devices: 658 us -> 72.2 us
  other arithmetic: 298 us -> 2.38 us
  Pallas kernels: 0 us -> 63.6 us
  matrix products: 38.5 us -> 0.38 us
  between operations: 14.7 us -> 0.72 us
  blocking collectives: 0 us -> 13.8 us
    ppermute x21 -> x29, waiting for transfers between devices: 504 us -> 55.5 us  [the longest x8 50 us: over_y(): lax.ppermute(x, 'tp', [(i, (i + 2 * shift) % n_tp) for i in range(n_tp)])]
    dot_general x18 -> x0, other arithmetic: 253 us -> none  [the longest x12 137 us: body(): jnp.einsum('shc,shdc->hdc', weights[offset], shifted, preferred_element_t...]
    reduce_scatter x3 -> x0, waiting for transfers between devices: 91.6 us -> none  [body(): lax.psum_scatter(lax.dot_general(w_layer, mixed_out, (((0,), (0,)), ((),...]
    pallas_call x0 -> x29, Pallas kernels: none -> 63.6 us  [call(): pl.pallas_call(kernel, in_specs=[smem] * len(scalars) + [vmem] * len(args...]
    all_gather x3 -> x0, waiting for transfers between devices: 61.9 us -> none  [body(): lax.all_gather(current, 'tp', axis=1, tiled=True)[0].astype(jnp.float32)]
    dot_general x9 -> x1, matrix products: 38.5 us -> 0.38 us  [dense_bias(): base = jnp.dot(flat, pick.astype(F32), precision=lax.Precision.HIGHEST)]
    convert_element_type x9 -> x0, other arithmetic: 25.6 us -> none  [the longest x3 19.2 us: body(): mixed_out = mixed_out.reshape(channels, columns).astype(jnp.bfloat16)]
    unnamed x65 -> x77, local copies, waits for them, and re-layouts: 5.68 us -> 22.4 us
  transfers between devices with their start and end apart: 27 -> 32, of which waited for: 15 -> 11; matrix products, arithmetic and copies ran while one was open for 3% -> 0% of each run, Pallas kernels for 0% -> 26%
where the time goes in v2:
time: 212 us; the launch traced here: 211 us
  waiting for transfers between devices  72.2 us (34%)
  Pallas kernels  63.6 us (30%)
  starting transfers between devices  33.4 us (16%)
  local copies, waits for them, and re-layouts  24.9 us (12%)
  blocking collectives  13.8 us (7%)
  other arithmetic  2.38 us (1%)
    pallas_call x29, Pallas kernels, call(): pl.pallas_call(kernel, in_specs=[smem] * len(scalars) + [vmem] * len(args...  63.6 us
    ppermute x8, waiting for transfers between devices, over_y(): lax.ppermute(x, 'tp', [(i, (i + 2 * shift) % n_tp) for i in range(n_tp)])  50 us
    unnamed x77, local copies, waits for them, and re-layouts  22.4 us
    all_to_all x2, waiting for transfers between devices, body(): got = lax.all_to_all(send, 'sp', 0, 0, tiled=True)  16.7 us
    all_to_all x1, blocking collectives, body(): fresh.append(lax.all_to_all(done, 'sp', 0, 0, tiled=True))  13.8 us
    all_to_all x2, starting transfers between devices, body(): got = lax.all_to_all(send, 'sp', 0, 0, tiled=True)  10.4 us
    ppermute x8, starting transfers between devices, over_y(): lax.ppermute(x, 'tp', [(i, (i + 2 * shift) % n_tp) for i in range(n_tp)])  9.57 us
  transfers between devices with their start and end apart: 32, of which 11 were waited for; matrix products, arithmetic and copies ran while one was open for 0% of the time, Pallas kernels for 26%

profile of v2, /device:TPU:0, one launch (start us, length us, event | category | flops | bytes accessed | tf_op | source)
XLA Modules:
  0.0 211.4 jit_solution(13918464472111515292)
XLA Ops:
  0.0 2.3 %dynamic-slice_bitcast_fusion.1 = (bf16[1,3,512,512]{3,2,1,0:T(8,128)(2,1)S(1)}, bf16[1,3,512,512]{3,2,1,0:T(8,128)(2,1)S(1)}) fusion(bf16[3,512,2048]{2,1,0:T(8,128)(2,1)} %w_out_ref.11, s32[]{:T(128)S(6)} %select_n.90, s32[]{:T(128)S(6)} %select_n.91), kind=kLoop, calls=%fused_computation.2 | loop fusion | bytes 6291464 | tf_op jit(solution)/shard_map/stack | solution.py:385
  2.3 1.9 pad_maximum_fusion
  4.7 3.2 %split_columns.1 = (bf16[8,32,512]{2,1,0:T(8,128)(2,1)}, bf16[8,32,512]{2,1,0:T(8,128)(2,1)}) custom-call(bf16[512,512]{1,0:T(8,128)(2,1)S(1)} %bitcast.32), custom_call_target="tpu_custom_call" | custom-call | tf_op jit(solution)/shard_map/split_columns/pallas_call | solution.py:31
  8.0 6.8 %all-to-all-start.1 = ((bf16[8,32,512]{2,1,0:T(8,128)(2,1)}), bf16[8,32,512]{2,1,0:T(8,128)(2,1)S(1)}, u32[]{:S(2)}, u32[]{:S(2)}) async-start(bf16[8,32,512]{2,1,0:T(8,128)(2,1)} %get-tuple-element.39), calls=%async_computation.1 | async-start | bytes 524288 | tf_op jit(solution)/shard_map/all_to_all | solution.py:378
  14.9 9.5 %all-to-all-done.1.x_ref = bf16[8,32,512]{2,1,0:T(8,128)(2,1)S(1)} async-done(((bf16[8,32,512]{2,1,0:T(8,128)(2,1)}), bf16[8,32,512]{2,1,0:T(8,128)(2,1)S(1)}, u32[]{:S(2)}, u32[]{:S(2)}) %all-to-all-start.1) | async-done | bytes 262176 | tf_op jit(solution)/shard_map/all_to_all | solution.py:378
  24.4 3.6 %all-to-all-start = ((bf16[8,32,512]{2,1,0:T(8,128)(2,1)}), bf16[8,32,512]{2,1,0:T(8,128)(2,1)S(1)}, u32[]{:S(2)}, u32[]{:S(2)}) async-start(bf16[8,32,512]{2,1,0:T(8,128)(2,1)} %get-tuple-element.35), calls=%async_computation | async-start | bytes 524288 | tf_op jit(solution)/shard_map/all_to_all | solution.py:378
  28.2 1.6 collective-permute-start.3
  29.9 7.2 %all-to-all-done.x_ref = bf16[8,32,512]{2,1,0:T(8,128)(2,1)S(1)} async-done(((bf16[8,32,512]{2,1,0:T(8,128)(2,1)}), bf16[8,32,512]{2,1,0:T(8,128)(2,1)S(1)}, u32[]{:S(2)}, u32[]{:S(2)}) %all-to-all-start) | async-done | bytes 262176 | tf_op jit(solution)/shard_map/all_to_all | solution.py:378
  37.1 0.9 to_column_order.2.refs_0_
  38.0 1.5 collective-permute-start
  40.4 4.4 %collective-permute-done.refs_1_ = bf16[256,512]{1,0:T(8,128)(2,1)} collective-permute-done((bf16[256,512]{1,0:T(8,128)(2,1)}, bf16[256,512]{1,0:T(8,128)(2,1)}, u32[]{:S(2)}, u32[]{:S(2)}) %collective-permute-start) | collective-permute-done | bytes 262176 | tf_op jit(solution)/shard_map/ppermute | solution.py:372
  44.8 2.8 %copy-done.2 = bf16[3,2048,512]{2,1,0:T(8,128)(2,1)S(1)} copy-done((bf16[3,2048,512]{2,1,0:T(8,128)(2,1)S(1)}, bf16[3,2048,512]{2,1,0:T(8,128)(2,1)}, u32[]{:S(2)}) %copy-start.2) | copy-done | bytes 6291480
  47.6 2.8 %copy-done.5 = bf16[3,2048,512]{2,1,0:T(8,128)(2,1)S(1)} copy-done((bf16[3,2048,512]{2,1,0:T(8,128)(2,1)S(1)}, bf16[3,2048,512]{2,1,0:T(8,128)(2,1)}, u32[]{:S(2)}) %copy-start.5) | copy-done | bytes 6291480
  50.4 2.8 %copy-done.7 = bf16[3,2048,512]{2,1,0:T(8,128)(2,1)S(1)} copy-done((bf16[3,2048,512]{2,1,0:T(8,128)(2,1)S(1)}, bf16[3,2048,512]{2,1,0:T(8,128)(2,1)}, u32[]{:S(2)}) %copy-start.7) | copy-done | bytes 6291480
  53.2 2.6 %qkv.7 = (bf16[256,512]{1,0:T(8,128)(2,1)S(1)}, bf16[256,512]{1,0:T(8,128)(2,1)S(1)}, bf16[256,512]{1,0:T(8,128)(2,1)S(1)}, bf16[2,64,512]{2,1,0:T(8,128)(2,1)S(1)}, bf16[2,64,512]{2,1,0:T(8,128)(2,1)S(1)}) custom-call(s32[4]{0:T(128)S(1)} %pad_add_fusion.1.ids_ref, bf16[256,512]{1,0:T(8,128)(2,1)S(1)} %to_column_order.3.refs_0_, ...), custom_call_target="tpu_custom_call" | custom-call | tf_op jit(solution)/shard_map/qkv/pallas_call | solution.py:31
  55.8 1.0 collective-permute-start.10
  56.8 1.1 collective-permute-start.11
  58.3 2.4 %expand_bias.1.refs_4_.refs_6_ = f32[24,128,256]{2,1,0:T(8,128)S(1)} custom-call(f32[24,8,256]{2,1,0:T(8,128)S(1)} %pad.4.base_ref), custom_call_target="tpu_custom_call" | custom-call | tf_op jit(solution)/shard_map/expand_bias/pallas_call | solution.py:31
  60.8 3.3 %qkv.6 = (bf16[256,512]{1,0:T(8,128)(2,1)S(1)}, bf16[256,512]{1,0:T(8,128)(2,1)S(1)}, bf16[256,512]{1,0:T(8,128)(2,1)S(1)}) custom-call(s32[4]{0:T(128)S(1)} %pad_add_fusion.1.ids_ref, bf16[256,512]{1,0:T(8,128)(2,1)} %to_column_order.2.refs_0_, bf16[256,512]{1,0:T(8,128)(2,1)} %collective-permute-done.refs_1_, ...), custom_call_target="tpu_custom_call" | custom-call | tf_op jit(solution)/shard_map/qkv/pallas_call | solution.py:31
  64.1 2.0 attention.7.own_ref
  66.2 2.0 attention.6.own_ref
  68.8 2.6 %project.7.refs_2_ = bf16[256,1024]{1,0:T(8,128)(2,1)S(1)} custom-call(s32[2]{0:T(128)S(1)} %iota.80.ys_ref, s32[1]{0:T(128)} %bitcast.4.core_ref, bf16[256,512]{1,0:T(8,128)(2,1)S(1)} %attention.7.own_ref, bf16[256,512]{1,0:T(8,128)(2,1)S(1)} %collective-permute-done.12.other_ref, bf16[3,512,2048]{2,1,0:T(8,128)(2,1)S(1)} %bitcast.25, ...), custom_call_target="tpu_custom_call" | custom-call | tf_op jit(solution)/shard_map/project/pallas_call | solution.py:31
  71.4 1.6 collective-permute-start.13
  73.0 2.7 %project.6.refs_2_ = bf16[256,1024]{1,0:T(8,128)(2,1)S(1)} custom-call(s32[2]{0:T(128)S(1)} %iota.61.ys_ref, s32[1]{0:T(128)} %bitcast.4.core_ref, bf16[256,512]{1,0:T(8,128)(2,1)S(1)} %attention.6.own_ref, bf16[256,512]{1,0:T(8,128)(2,1)S(1)} %collective-permute-done.6.other_ref, bf16[3,512,2048]{2,1,0:T(8,128)(2,1)S(1)} %bitcast.25, ...), custom_call_target="tpu_custom_call" | custom-call | tf_op jit(solution)/shard_map/project/pallas_call | solution.py:31
  76.3 10.0 %collective-permute-done.13.refs_3_ = bf16[256,1024]{1,0:T(8,128)(2,1)S(1)} collective-permute-done((bf16[256,1024]{1,0:T(8,128)(2,1)S(1)}, bf16[256,1024]{1,0:T(8,128)(2,1)S(1)}, u32[]{:S(2)}, u32[]{:S(2)}) %collective-permute-start.13) | collective-permute-done | bytes 524320 | tf_op jit(solution)/shard_map/ppermute | solution.py:372
  86.3 1.6 add_update.5.refs_0_
  87.9 8.7 %collective-permute-done.8.refs_3_ = bf16[256,1024]{1,0:T(8,128)(2,1)S(1)} collective-permute-done((bf16[256,1024]{1,0:T(8,128)(2,1)S(1)}, bf16[256,1024]{1,0:T(8,128)(2,1)S(1)}, u32[]{:S(2)}, u32[]{:S(2)}) %collective-permute-start.8) | collective-permute-done | bytes 524320 | tf_op jit(solution)/shard_map/ppermute | solution.py:372
  96.6 2.1 %add_update.4.refs_0_ = bf16[256,1024]{1,0:T(8,128)(2,1)} custom-call(s32[2]{0:T(128)S(1)} %pad_add_fusion.where_ref, bf16[256,512]{1,0:T(8,128)(2,1)} %to_column_order.2.refs_0_, bf16[256,512]{1,0:T(8,128)(2,1)} %collective-permute-done.refs_1_, bf16[256,1024]{1,0:T(8,128)(2,1)S(1)} %project.6.refs_2_, bf16[256,1024]{1,0:T(8,128)(2,1)S(1)} %collective-permute-done.8.refs_3_), custom_call_target="tpu_custom_call" | custom-call | tf_op jit(solution)/shard_map/add_update/pallas_call | solution.py:31
  98.8 2.8 %copy-done.4 = bf16[3,2048,512]{2,1,0:T(8,128)(2,1)S(1)} copy-done((bf16[3,2048,512]{2,1,0:T(8,128)(2,1)S(1)}, bf16[3,2048,512]{2,1,0:T(8,128)(2,1)}, u32[]{:S(2)}) %copy-start.4) | copy-done | bytes 6291480
  101.6 2.8 %copy-done.6 = bf16[3,2048,512]{2,1,0:T(8,128)(2,1)S(1)} copy-done((bf16[3,2048,512]{2,1,0:T(8,128)(2,1)S(1)}, bf16[3,2048,512]{2,1,0:T(8,128)(2,1)}, u32[]{:S(2)}) %copy-start.6) | copy-done | bytes 6291480
  104.4 2.8 %copy-done.8 = bf16[3,2048,512]{2,1,0:T(8,128)(2,1)S(1)} copy-done((bf16[3,2048,512]{2,1,0:T(8,128)(2,1)S(1)}, bf16[3,2048,512]{2,1,0:T(8,128)(2,1)}, u32[]{:S(2)}) %copy-start.8) | copy-done | bytes 6291480
  107.2 3.4 %qkv.9 = (bf16[256,512]{1,0:T(8,128)(2,1)S(1)}, bf16[256,512]{1,0:T(8,128)(2,1)S(1)}, bf16[256,512]{1,0:T(8,128)(2,1)S(1)}, bf16[2,64,512]{2,1,0:T(8,128)(2,1)S(1)}, bf16[2,64,512]{2,1,0:T(8,128)(2,1)S(1)}) custom-call(s32[4]{0:T(128)S(1)} %pad_add_fusion.2.ids_ref, bf16[256,1024]{1,0:T(8,128)(2,1)} %add_update.5.refs_0_, ...), custom_call_target="tpu_custom_call" | custom-call | tf_op jit(solution)/shard_map/qkv/pallas_call | solution.py:31
  110.6 1.0 collective-permute-start.18
  111.6 1.1 collective-permute-start.19
  112.7 3.5 %qkv.8 = (bf16[256,512]{1,0:T(8,128)(2,1)S(1)}, bf16[256,512]{1,0:T(8,128)(2,1)S(1)}, bf16[256,512]{1,0:T(8,128)(2,1)S(1)}) custom-call(s32[4]{0:T(128)S(1)} %pad_add_fusion.2.ids_ref, bf16[256,1024]{1,0:T(8,128)(2,1)} %add_update.4.refs_0_, bf16[256,1024]{1,0:T(8,128)(2,1)} %collective-permute-done.9.refs_1_, f32[3,4,1,512]{3,2,1,0:T(1,128)S(1)} %reshape.29.refs_4_.refs_2_, ...), custom_call_target="tpu_custom_call" | custom-call | tf_op jit(solution)/shard_map/qkv/pallas_call | solution.py:31
  116.2 2.0 attention.8.own_ref
  118.4 2.0 attention.9.own_ref
  120.9 2.8 %project.8.refs_1_ = bf16[256,1024]{1,0:T(8,128)(2,1)S(1)} custom-call(s32[2]{0:T(128)S(1)} %iota.79.ys_ref, s32[1]{0:T(128)} %bitcast.4.core_ref, bf16[256,512]{1,0:T(8,128)(2,1)S(1)} %attention.8.own_ref, bf16[256,512]{1,0:T(8,128)(2,1)S(1)} %collective-permute-done.15.other_ref, bf16[3,512,2048]{2,1,0:T(8,128)(2,1)S(1)} %bitcast.27, ...), custom_call_target="tpu_custom_call" | custom-call | tf_op jit(solution)/shard_map/project/pallas_call | solution.py:31
  123.7 1.6 collective-permute-start.16
  125.3 2.8 %project.9.refs_1_ = bf16[256,1024]{1,0:T(8,128)(2,1)S(1)} custom-call(s32[2]{0:T(128)S(1)} %iota.81.ys_ref, s32[1]{0:T(128)} %bitcast.4.core_ref, bf16[256,512]{1,0:T(8,128)(2,1)S(1)} %attention.9.own_ref, bf16[256,512]{1,0:T(8,128)(2,1)S(1)} %collective-permute-done.20.other_ref, bf16[3,512,2048]{2,1,0:T(8,128)(2,1)S(1)} %bitcast.27, ...), custom_call_target="tpu_custom_call" | custom-call | tf_op jit(solution)/shard_map/project/pallas_call | solution.py:31
  128.6 9.9 %collective-permute-done.16.refs_2_ = bf16[256,1024]{1,0:T(8,128)(2,1)S(1)} collective-permute-done((bf16[256,1024]{1,0:T(8,128)(2,1)S(1)}, bf16[256,1024]{1,0:T(8,128)(2,1)S(1)}, u32[]{:S(2)}, u32[]{:S(2)}) %collective-permute-start.16) | collective-permute-done | bytes 524320 | tf_op jit(solution)/shard_map/ppermute | solution.py:372
  138.5 1.2 add_update.6.refs_0_.old_ref
  139.9 9.1 %collective-permute-done.21.refs_2_ = bf16[256,1024]{1,0:T(8,128)(2,1)S(1)} collective-permute-done((bf16[256,1024]{1,0:T(8,128)(2,1)S(1)}, bf16[256,1024]{1,0:T(8,128)(2,1)S(1)}, u32[]{:S(2)}, u32[]{:S(2)}) %collective-permute-start.21) | collective-permute-done | bytes 524320 | tf_op jit(solution)/shard_map/ppermute | solution.py:372
  148.9 1.2 add_update.7.refs_0_.old_ref
  150.3 2.6 %qkv.10 = (bf16[256,512]{1,0:T(8,128)(2,1)S(1)}, bf16[256,512]{1,0:T(8,128)(2,1)S(1)}, bf16[256,512]{1,0:T(8,128)(2,1)S(1)}) custom-call(s32[4]{0:T(128)S(1)} %pad_add_fusion.2.ids_ref, bf16[256,1024]{1,0:T(8,128)(2,1)S(1)} %add_update.6.refs_0_.old_ref, bf16[256,1024]{1,0:T(8,128)(2,1)S(1)} %collective-permute-done.17.refs_1_, ...), custom_call_target="tpu_custom_call" | custom-call | tf_op jit(solution)/shard_map/qkv/pallas_call | solution.py:31
  153.0 2.6 %qkv.11 = (bf16[256,512]{1,0:T(8,128)(2,1)S(1)}, bf16[256,512]{1,0:T(8,128)(2,1)S(1)}, bf16[256,512]{1,0:T(8,128)(2,1)S(1)}, bf16[2,64,512]{2,1,0:T(8,128)(2,1)S(1)}, bf16[2,64,512]{2,1,0:T(8,128)(2,1)S(1)}) custom-call(s32[4]{0:T(128)S(1)} %pad_add_fusion.2.ids_ref, bf16[256,1024]{1,0:T(8,128)(2,1)S(1)} %add_update.7.refs_0_.old_ref, ...), custom_call_target="tpu_custom_call" | custom-call | tf_op jit(solution)/shard_map/qkv/pallas_call | solution.py:31
  155.8 2.7 %attention.10.own_ref = bf16[256,512]{1,0:T(8,128)(2,1)} custom-call(bf16[256,512]{1,0:T(8,128)(2,1)S(1)} %get-tuple-element.50.q_ref, bf16[256,512]{1,0:T(8,128)(2,1)S(1)} %get-tuple-element.51.refs_0_, bf16[256,512]{1,0:T(8,128)(2,1)S(1)} %get-tuple-element.52.refs_1_, bf16[256,512]{1,0:T(8,128)(2,1)S(1)} %get-tuple-element.56.refs_2_, ...), custom_call_target="tpu_custom_call" | custom-call | tf_op jit(solution)/shard_map/attention/pallas_call | solution.py:31
  159.1 1.4 collective-permute-done.23.other_ref
  160.5 2.8 %copy-done = bf16[3,512,2048]{2,1,0:T(8,128)(2,1)S(1)} copy-done((bf16[3,512,2048]{2,1,0:T(8,128)(2,1)S(1)}, bf16[3,512,2048]{2,1,0:T(8,128)(2,1)}, u32[]{:S(2)}) %copy-start) | copy-done | bytes 6291480
  163.4 2.9 %project.10 = (bf16[256,512]{1,0:T(8,128)(2,1)S(1)}, bf16[256,512]{1,0:T(8,128)(2,1)S(1)}) custom-call(s32[2]{0:T(128)S(1)} %pad_add_fusion.3.ys_ref, s32[1]{0:T(128)} %bitcast.4.core_ref, bf16[256,512]{1,0:T(8,128)(2,1)} %attention.10.own_ref, bf16[256,512]{1,0:T(8,128)(2,1)} %collective-permute-done.23.other_ref, bf16[3,512,2048]{2,1,0:T(8,128)(2,1)S(1)} %copy-done, ...), custom_call_target="tpu_custom_call" | custom-call | tf_op jit(solution)/shard_map/project/pallas_call | solution.py:31
  166.2 1.6 collective-permute-start.24
  167.8 0.9 collective-permute-start.25
  168.7 1.2 collective-permute-start.26
  169.9 3.5 %collective-permute-done.25.refs_4_ = bf16[2,64,512]{2,1,0:T(8,128)(2,1)S(1)} collective-permute-done((bf16[2,64,512]{2,1,0:T(8,128)(2,1)S(1)}, bf16[2,64,512]{2,1,0:T(8,128)(2,1)S(1)}, u32[]{:S(2)}, u32[]{:S(2)}) %collective-permute-start.25) | collective-permute-done | bytes 131104 | tf_op jit(solution)/shard_map/ppermute | solution.py:415
  173.3 0.6 collective-permute-done.26.refs_5_
  173.9 2.7 %attention.11.own_ref = bf16[256,512]{1,0:T(8,128)(2,1)} custom-call(bf16[256,512]{1,0:T(8,128)(2,1)S(1)} %copy-done.23, bf16[256,512]{1,0:T(8,128)(2,1)S(1)} %get-tuple-element.51.refs_0_, bf16[256,512]{1,0:T(8,128)(2,1)S(1)} %copy-done.16, bf16[256,512]{1,0:T(8,128)(2,1)S(1)} %copy-done.18, bf16[256,512]{1,0:T(8,128)(2,1)S(1)} %copy-done.20, ...), custom_call_target="tpu_custom_call" | custom-call | tf_op jit(solution)/shard_map/attention/pallas_call | solution.py:31
  176.6 1.0 finish.2
  177.7 4.2 %all-to-all-start.2 = ((bf16[8,32,512]{2,1,0:T(8,128)(2,1)}), bf16[8,32,512]{2,1,0:T(8,128)(2,1)S(1)}, u32[]{:S(2)}, u32[]{:S(2)}) async-start(bf16[8,32,512]{2,1,0:T(8,128)(2,1)} %finish.2), calls=%async_computation.2 | async-start | bytes 524288 | tf_op jit(solution)/shard_map/all_to_all | solution.py:453
  181.9 2.8 %copy-done.1 = bf16[3,512,2048]{2,1,0:T(8,128)(2,1)S(1)} copy-done((bf16[3,512,2048]{2,1,0:T(8,128)(2,1)S(1)}, bf16[3,512,2048]{2,1,0:T(8,128)(2,1)}, u32[]{:S(2)}) %copy-start.1) | copy-done | bytes 6291480
  184.7 2.7 %project.11 = (bf16[256,512]{1,0:T(8,128)(2,1)S(1)}, bf16[256,512]{1,0:T(8,128)(2,1)S(1)}) custom-call(s32[2]{0:T(128)S(1)} %pad_add_fusion.3.ys_ref, s32[1]{0:T(128)} %bitcast.4.core_ref, bf16[256,512]{1,0:T(8,128)(2,1)} %attention.11.own_ref, bf16[256,512]{1,0:T(8,128)(2,1)S(1)} %collective-permute-done.27.other_ref, bf16[3,512,2048]{2,1,0:T(8,128)(2,1)S(1)} %copy-done.1, ...), custom_call_target="tpu_custom_call" | custom-call | tf_op jit(solution)/shard_map/project/pallas_call | solution.py:31
  187.4 0.6 collective-permute-start.28
  188.0 7.9 %collective-permute-done.28.refs_1_ = bf16[256,512]{1,0:T(8,128)(2,1)S(1)} collective-permute-done((bf16[256,512]{1,0:T(8,128)(2,1)S(1)}, bf16[256,512]{1,0:T(8,128)(2,1)S(1)}, u32[]{:S(2)}, u32[]{:S(2)}) %collective-permute-start.28) | collective-permute-done | bytes 262176 | tf_op jit(solution)/shard_map/ppermute | solution.py:372
  196.3 13.8 %all_to_all.20.refs_1_ = bf16[8,32,512]{2,1,0:T(8,128)(2,1)S(1)} all-to-all(bf16[8,32,512]{2,1,0:T(8,128)(2,1)S(1)} %finish.3), channel_id=1, replica_groups=mesh['sp'=8,'tp'=4] {'sp'}, dimensions={0} | all-to-all | bytes 524288 | tf_op jit(solution)/shard_map/all_to_all | solution.py:453
  210.1 1.3 merge_columns.1
  (137 shorter events, 6.0 us)
Async XLA Ops:
  2.3 12.5 %copy-start.28 = (f32[3,8,8,16]{3,2,1,0:T(8,128)S(1)}, f32[3,8,8,16]{3,2,1,0:T(8,128)}, u32[]{:S(2)}) copy-start(f32[3,8,8,16]{3,2,1,0:T(8,128)} %param.13) | copy-start | bytes 36868
  4.2 35.4 %copy-start.29 = (bf16[3,2048]{1,0:T(4,128)(2,1)S(1)}, bf16[3,2048]{1,0:T(4,128)(2,1)}, u32[]{:S(2)}) copy-start(bf16[3,2048]{1,0:T(4,128)(2,1)} %param.8) | copy-start | bytes 36868
  4.2 64.5 %collective-permute-start.7 = (bf16[2,3,512,512]{3,2,1,0:T(8,128)(2,1)}, bf16[2,3,512,512]{3,2,1,0:T(8,128)(2,1)}, u32[]{:S(2)}, u32[]{:S(2)}) collective-permute-start(bf16[2,3,512,512]{3,2,1,0:T(8,128)(2,1)} %pad_maximum_fusion), channel_id=1, source_target_pairs={{0,1},{1,0},{2,3},{3,2},{4,5},{5,4},{6,7},{7,6},{8,9},{9,8},{10,11... | collective-permute-start | bytes 9437192 | tf_op jit(solution)/shard_map/ppermute | solution.py:369
  8.0 16.4 %all-to-all-start.1 = ((bf16[8,32,512]{2,1,0:T(8,128)(2,1)}), bf16[8,32,512]{2,1,0:T(8,128)(2,1)S(1)}, u32[]{:S(2)}, u32[]{:S(2)}) async-start(bf16[8,32,512]{2,1,0:T(8,128)(2,1)} %get-tuple-element.39), calls=%async_computation.1 | async-start | bytes 524288 | tf_op jit(solution)/shard_map/all_to_all | solution.py:378
  24.4 12.7 %all-to-all-start = ((bf16[8,32,512]{2,1,0:T(8,128)(2,1)}), bf16[8,32,512]{2,1,0:T(8,128)(2,1)S(1)}, u32[]{:S(2)}, u32[]{:S(2)}) async-start(bf16[8,32,512]{2,1,0:T(8,128)(2,1)} %get-tuple-element.35), calls=%async_computation | async-start | bytes 524288 | tf_op jit(solution)/shard_map/all_to_all | solution.py:378
  28.2 11.3 %collective-permute-start.3 = (bf16[256,512]{1,0:T(8,128)(2,1)S(1)}, bf16[256,512]{1,0:T(8,128)(2,1)S(1)}, u32[]{:S(2)}, u32[]{:S(2)}) collective-permute-start(bf16[256,512]{1,0:T(8,128)(2,1)S(1)} %to_column_order.3.refs_0_), channel_id=1, source_target_pairs={{0,2},{1,3},{2,0},{3,1},{4,6},{5,7},{6,4},{7,5},{8,10},{9,11},{10,... | collective-permute-start | bytes 786440 | tf_op jit(solution)/shard_map/ppermute | solution.py:372
  29.8 15.0 %collective-permute-start.4 = (bf16[256,512]{1,0:T(8,128)(2,1)S(1)}, bf16[256,512]{1,0:T(8,128)(2,1)S(1)}, u32[]{:S(2)}, u32[]{:S(2)}) collective-permute-start(bf16[256,512]{1,0:T(8,128)(2,1)S(1)} %to_column_order.3.refs_0_), channel_id=1, source_target_pairs={{0,1},{1,0},{2,3},{3,2},{4,5},{5,4},{6,7},{7,6},{8,9},{9,8},{10,11... | collective-permute-start | bytes 786440 | tf_op jit(solution)/shard_map/ppermute | solution.py:369
  38.0 6.8 %collective-permute-start = (bf16[256,512]{1,0:T(8,128)(2,1)}, bf16[256,512]{1,0:T(8,128)(2,1)}, u32[]{:S(2)}, u32[]{:S(2)}) collective-permute-start(bf16[256,512]{1,0:T(8,128)(2,1)} %to_column_order.2.refs_0_), channel_id=1, source_target_pairs={{0,2},{1,3},{2,0},{3,1},{4,6},{5,7},{6,4},{7,5},{8,10},{9,11},{10,... | collective-permute-start | bytes 786440 | tf_op jit(solution)/shard_map/ppermute | solution.py:372
  39.5 16.3 %copy-start.13 = (bf16[256,512]{1,0:T(8,128)(2,1)}, bf16[256,512]{1,0:T(8,128)(2,1)S(1)}, u32[]{:S(2)}) copy-start(bf16[256,512]{1,0:T(8,128)(2,1)S(1)} %collective-permute-done.3.refs_1_) | copy-start | bytes 786436
  39.5 5.3 %collective-permute-start.5 = (bf16[256,512]{1,0:T(8,128)(2,1)S(1)}, bf16[256,512]{1,0:T(8,128)(2,1)S(1)}, u32[]{:S(2)}, u32[]{:S(2)}) collective-permute-start(bf16[256,512]{1,0:T(8,128)(2,1)S(1)} %collective-permute-done.3.refs_1_), channel_id=1, source_target_pairs={{0,1},{1,0},{2,3},{3,2},{4,5},{5,4},{6,7},{7,6},{8,9},{9,8},{10,11... | collective-permute-start | bytes 786440 | tf_op jit(solution)/shard_map/ppermute | solution.py:369
  39.8 20.9 %collective-permute-start.1 = (bf16[256,512]{1,0:T(8,128)(2,1)}, bf16[256,512]{1,0:T(8,128)(2,1)S(1)}, u32[]{:S(2)}, u32[]{:S(2)}) collective-permute-start(bf16[256,512]{1,0:T(8,128)(2,1)} %to_column_order.2.refs_0_), channel_id=1, source_target_pairs={{0,1},{1,0},{2,3},{3,2},{4,5},{5,4},{6,7},{7,6},{8,9},{9,8},{10,11... | collective-permute-start | bytes 786440 | tf_op jit(solution)/shard_map/ppermute | solution.py:369
  44.8 16.0 %collective-permute-start.2 = (bf16[256,512]{1,0:T(8,128)(2,1)}, bf16[256,512]{1,0:T(8,128)(2,1)S(1)}, u32[]{:S(2)}, u32[]{:S(2)}) collective-permute-start(bf16[256,512]{1,0:T(8,128)(2,1)} %collective-permute-done.refs_1_), channel_id=1, source_target_pairs={{0,1},{1,0},{2,3},{3,2},{4,5},{5,4},{6,7},{7,6},{8,9},{9,8},{10,11... | collective-permute-start | bytes 786440 | tf_op jit(solution)/shard_map/ppermute | solution.py:369
  44.8 2.8 %copy-start.2 = (bf16[3,2048,512]{2,1,0:T(8,128)(2,1)S(1)}, bf16[3,2048,512]{2,1,0:T(8,128)(2,1)}, u32[]{:S(2)}) copy-start(bf16[3,2048,512]{2,1,0:T(8,128)(2,1)} %refs_3_.7) | copy-start | bytes 18874372
  47.6 2.8 %copy-start.5 = (bf16[3,2048,512]{2,1,0:T(8,128)(2,1)S(1)}, bf16[3,2048,512]{2,1,0:T(8,128)(2,1)}, u32[]{:S(2)}) copy-start(bf16[3,2048,512]{2,1,0:T(8,128)(2,1)} %refs_4_.7) | copy-start | bytes 18874372
  50.4 2.8 %copy-start.7 = (bf16[3,2048,512]{2,1,0:T(8,128)(2,1)S(1)}, bf16[3,2048,512]{2,1,0:T(8,128)(2,1)}, u32[]{:S(2)}) copy-start(bf16[3,2048,512]{2,1,0:T(8,128)(2,1)} %refs_5_.11) | copy-start | bytes 18874372
  55.8 8.3 %collective-permute-start.10 = (bf16[2,64,512]{2,1,0:T(8,128)(2,1)S(1)}, bf16[2,64,512]{2,1,0:T(8,128)(2,1)S(1)}, u32[]{:S(2)}, u32[]{:S(2)}) collective-permute-start(bf16[2,64,512]{2,1,0:T(8,128)(2,1)S(1)} %get-tuple-element.46), channel_id=1, source_target_pairs={{0,8},{8,16},{16,24},{24,28},{28,20},{20,12},{12,4},{4,0},{1,9},{9... | collective-permute-start | bytes 393224 | tf_op jit(solution)/shard_map/ppermute | solution.py:415
  56.8 7.3 %collective-permute-start.11 = (bf16[2,64,512]{2,1,0:T(8,128)(2,1)S(1)}, bf16[2,64,512]{2,1,0:T(8,128)(2,1)S(1)}, u32[]{:S(2)}, u32[]{:S(2)}) collective-permute-start(bf16[2,64,512]{2,1,0:T(8,128)(2,1)S(1)} %get-tuple-element.47), channel_id=1, source_target_pairs={{8,0},{16,8},{24,16},{28,24},{20,28},{12,20},{4,12},{0,4},{9,1},{1... | collective-permute-start | bytes 393224 | tf_op jit(solution)/shard_map/ppermute | solution.py:414
  57.9 2.9 %copy-start.3 = (bf16[3,2048,512]{2,1,0:T(8,128)(2,1)S(1)}, bf16[3,2048,512]{2,1,0:T(8,128)(2,1)}, u32[]{:S(2)}) copy-start(bf16[3,2048,512]{2,1,0:T(8,128)(2,1)} %refs_3_.7) | copy-start | bytes 18874372
  58.3 10.5 %slice-start = ((s8[6291456]{0:T(1024)(128)(4,1)}), s8[4194304]{0:T(1024)(128)(4,1)S(1)}, s32[]{:S(2)}) async-start(s8[6291456]{0:T(1024)(128)(4,1)} %bitcast.24), calls=%async_computation.4 | async-start | bytes 8388608
  60.7 8.1 %slice-start.1 = ((s8[6291456]{0:T(1024)(128)(4,1)}), s8[2097152]{0:T(1024)(128)(4,1)S(1)}, s32[]{:S(2)}) async-start(s8[6291456]{0:T(1024)(128)(4,1)} %bitcast.24), calls=%async_computation.5 | async-start | bytes 4194304
  66.1 2.6 %collective-permute-start.12 = (bf16[256,512]{1,0:T(8,128)(2,1)S(1)}, bf16[256,512]{1,0:T(8,128)(2,1)S(1)}, u32[]{:S(2)}, u32[]{:S(2)}) collective-permute-start(bf16[256,512]{1,0:T(8,128)(2,1)S(1)} %attention.7.own_ref), channel_id=1, source_target_pairs={{0,1},{1,0},{2,3},{3,2},{4,5},{5,4},{6,7},{7,6},{8,9},{9,8},{10,11... | collective-permute-start | bytes 786440 | tf_op jit(solution)/shard_map/ppermute | solution.py:369
  68.2 4.8 %collective-permute-start.6 = (bf16[256,512]{1,0:T(8,128)(2,1)S(1)}, bf16[256,512]{1,0:T(8,128)(2,1)S(1)}, u32[]{:S(2)}, u32[]{:S(2)}) collective-permute-start(bf16[256,512]{1,0:T(8,128)(2,1)S(1)} %attention.6.own_ref), channel_id=1, source_target_pairs={{0,1},{1,0},{2,3},{3,2},{4,5},{5,4},{6,7},{7,6},{8,9},{9,8},{10,11... | collective-permute-start | bytes 786440 | tf_op jit(solution)/shard_map/ppermute | solution.py:369
  71.4 14.9 %collective-permute-start.13 = (bf16[256,1024]{1,0:T(8,128)(2,1)S(1)}, bf16[256,1024]{1,0:T(8,128)(2,1)S(1)}, u32[]{:S(2)}, u32[]{:S(2)}) collective-permute-start(bf16[256,1024]{1,0:T(8,128)(2,1)S(1)} %project.7.refs_2_), channel_id=1, source_target_pairs={{0,2},{1,3},{2,0},{3,1},{4,6},{5,7},{6,4},{7,5},{8,10},{9,11},{10,... | collective-permute-start | bytes 1572872 | tf_op jit(solution)/shard_map/ppermute | solution.py:372
  73.0 13.3 %copy-start.14 = (bf16[256,512]{1,0:T(8,128)(2,1)S(1)}, bf16[256,512]{1,0:T(8,128)(2,1)}, u32[]{:S(2)}) copy-start(bf16[256,512]{1,0:T(8,128)(2,1)} %copy-done.13) | copy-start | bytes 786436
  75.7 20.9 %collective-permute-start.8 = (bf16[256,1024]{1,0:T(8,128)(2,1)S(1)}, bf16[256,1024]{1,0:T(8,128)(2,1)S(1)}, u32[]{:S(2)}, u32[]{:S(2)}) collective-permute-start(bf16[256,1024]{1,0:T(8,128)(2,1)S(1)} %project.6.refs_2_), channel_id=1, source_target_pairs={{0,2},{1,3},{2,0},{3,1},{4,6},{5,7},{6,4},{7,5},{8,10},{9,11},{10,... | collective-permute-start | bytes 1572872 | tf_op jit(solution)/shard_map/ppermute | solution.py:372
  87.9 10.9 %collective-permute-start.14 = (bf16[256,1024]{1,0:T(8,128)(2,1)}, bf16[256,1024]{1,0:T(8,128)(2,1)}, u32[]{:S(2)}, u32[]{:S(2)}) collective-permute-start(bf16[256,1024]{1,0:T(8,128)(2,1)} %add_update.5.refs_0_), channel_id=1, source_target_pairs={{0,1},{1,0},{2,3},{3,2},{4,5},{5,4},{6,7},{7,6},{8,9},{9,8},{10,11... | collective-permute-start | bytes 1572872 | tf_op jit(solution)/shard_map/ppermute | solution.py:369
  98.7 14.0 %collective-permute-start.9 = (bf16[256,1024]{1,0:T(8,128)(2,1)}, bf16[256,1024]{1,0:T(8,128)(2,1)}, u32[]{:S(2)}, u32[]{:S(2)}) collective-permute-start(bf16[256,1024]{1,0:T(8,128)(2,1)} %add_update.4.refs_0_), channel_id=1, source_target_pairs={{0,1},{1,0},{2,3},{3,2},{4,5},{5,4},{6,7},{7,6},{8,9},{9,8},{10,11... | collective-permute-start | bytes 1572872 | tf_op jit(solution)/shard_map/ppermute | solution.py:369
  98.8 2.8 %copy-start.4 = (bf16[3,2048,512]{2,1,0:T(8,128)(2,1)S(1)}, bf16[3,2048,512]{2,1,0:T(8,128)(2,1)}, u32[]{:S(2)}) copy-start(bf16[3,2048,512]{2,1,0:T(8,128)(2,1)} %refs_3_.7) | copy-start | bytes 18874372
  101.6 2.8 %copy-start.6 = (bf16[3,2048,512]{2,1,0:T(8,128)(2,1)S(1)}, bf16[3,2048,512]{2,1,0:T(8,128)(2,1)}, u32[]{:S(2)}) copy-start(bf16[3,2048,512]{2,1,0:T(8,128)(2,1)} %refs_4_.7) | copy-start | bytes 18874372
  104.4 2.8 %copy-start.8 = (bf16[3,2048,512]{2,1,0:T(8,128)(2,1)S(1)}, bf16[3,2048,512]{2,1,0:T(8,128)(2,1)}, u32[]{:S(2)}) copy-start(bf16[3,2048,512]{2,1,0:T(8,128)(2,1)} %refs_5_.11) | copy-start | bytes 18874372
  107.2 13.7 %slice-start.2 = ((s8[6291456]{0:T(1024)(128)(4,1)}), s8[2097152]{0:T(1024)(128)(4,1)S(1)}, s32[]{:S(2)}) async-start(s8[6291456]{0:T(1024)(128)(4,1)} %bitcast.26), calls=%async_computation.6 | async-start | bytes 4194304
  110.6 7.8 %collective-permute-start.18 = (bf16[2,64,512]{2,1,0:T(8,128)(2,1)S(1)}, bf16[2,64,512]{2,1,0:T(8,128)(2,1)S(1)}, u32[]{:S(2)}, u32[]{:S(2)}) collective-permute-start(bf16[2,64,512]{2,1,0:T(8,128)(2,1)S(1)} %get-tuple-element.54), channel_id=1, source_target_pairs={{0,8},{8,16},{16,24},{24,28},{28,20},{20,12},{12,4},{4,0},{1,9},{9... | collective-permute-start | bytes 393224 | tf_op jit(solution)/shard_map/ppermute | solution.py:415
  111.6 9.2 %slice-start.3 = ((s8[6291456]{0:T(1024)(128)(4,1)}), s8[4194304]{0:T(1024)(128)(4,1)S(1)}, s32[]{:S(2)}) async-start(s8[6291456]{0:T(1024)(128)(4,1)} %bitcast.26), calls=%async_computation.7 | async-start | bytes 8388608
  111.6 6.8 %collective-permute-start.19 = (bf16[2,64,512]{2,1,0:T(8,128)(2,1)S(1)}, bf16[2,64,512]{2,1,0:T(8,128)(2,1)S(1)}, u32[]{:S(2)}, u32[]{:S(2)}) collective-permute-start(bf16[2,64,512]{2,1,0:T(8,128)(2,1)S(1)} %get-tuple-element.55), channel_id=1, source_target_pairs={{8,0},{16,8},{24,16},{28,24},{20,28},{12,20},{4,12},{0,4},{9,1},{1... | collective-permute-start | bytes 393224 | tf_op jit(solution)/shard_map/ppermute | solution.py:414
  118.2 2.7 %collective-permute-start.15 = (bf16[256,512]{1,0:T(8,128)(2,1)S(1)}, bf16[256,512]{1,0:T(8,128)(2,1)S(1)}, u32[]{:S(2)}, u32[]{:S(2)}) collective-permute-start(bf16[256,512]{1,0:T(8,128)(2,1)S(1)} %attention.8.own_ref), channel_id=1, source_target_pairs={{0,1},{1,0},{2,3},{3,2},{4,5},{5,4},{6,7},{7,6},{8,9},{9,8},{10,11... | collective-permute-start | bytes 786440 | tf_op jit(solution)/shard_map/ppermute | solution.py:369
  120.4 4.8 %collective-permute-start.20 = (bf16[256,512]{1,0:T(8,128)(2,1)S(1)}, bf16[256,512]{1,0:T(8,128)(2,1)S(1)}, u32[]{:S(2)}, u32[]{:S(2)}) collective-permute-start(bf16[256,512]{1,0:T(8,128)(2,1)S(1)} %attention.9.own_ref), channel_id=1, source_target_pairs={{0,1},{1,0},{2,3},{3,2},{4,5},{5,4},{6,7},{7,6},{8,9},{9,8},{10,11... | collective-permute-start | bytes 786440 | tf_op jit(solution)/shard_map/ppermute | solution.py:369
  120.9 29.4 %slice-start.6 = ((s8[6291456]{0:T(1024)(128)(4,1)}), s8[4194304]{0:T(1024)(128)(4,1)S(1)}, s32[]{:S(2)}) async-start(s8[6291456]{0:T(1024)(128)(4,1)} %bitcast.30), calls=%async_computation.10 | async-start | bytes 8388608
  123.7 14.9 %collective-permute-start.16 = (bf16[256,1024]{1,0:T(8,128)(2,1)S(1)}, bf16[256,1024]{1,0:T(8,128)(2,1)S(1)}, u32[]{:S(2)}, u32[]{:S(2)}) collective-permute-start(bf16[256,1024]{1,0:T(8,128)(2,1)S(1)} %project.8.refs_1_), channel_id=1, source_target_pairs={{0,2},{1,3},{2,0},{3,1},{4,6},{5,7},{6,4},{7,5},{8,10},{9,11},{10,... | collective-permute-start | bytes 1572872 | tf_op jit(solution)/shard_map/ppermute | solution.py:372
  125.3 25.1 %slice-start.4 = ((s8[6291456]{0:T(1024)(128)(4,1)}), s8[4194304]{0:T(1024)(128)(4,1)S(1)}, s32[]{:S(2)}) async-start(s8[6291456]{0:T(1024)(128)(4,1)} %bitcast.28), calls=%async_computation.8 | async-start | bytes 8388608
  125.3 25.1 %slice-start.5 = ((s8[6291456]{0:T(1024)(128)(4,1)}), s8[2097152]{0:T(1024)(128)(4,1)S(1)}, s32[]{:S(2)}) async-start(s8[6291456]{0:T(1024)(128)(4,1)} %bitcast.28), calls=%async_computation.9 | async-start | bytes 4194304
  125.3 25.1 %slice-start.7 = ((s8[6291456]{0:T(1024)(128)(4,1)}), s8[2097152]{0:T(1024)(128)(4,1)S(1)}, s32[]{:S(2)}) async-start(s8[6291456]{0:T(1024)(128)(4,1)} %bitcast.30), calls=%async_computation.11 | async-start | bytes 4194304
  128.1 20.9 %collective-permute-start.21 = (bf16[256,1024]{1,0:T(8,128)(2,1)S(1)}, bf16[256,1024]{1,0:T(8,128)(2,1)S(1)}, u32[]{:S(2)}, u32[]{:S(2)}) collective-permute-start(bf16[256,1024]{1,0:T(8,128)(2,1)S(1)} %project.9.refs_1_), channel_id=1, source_target_pairs={{0,2},{1,3},{2,0},{3,1},{4,6},{5,7},{6,4},{7,5},{8,10},{9,11},{10,... | collective-permute-start | bytes 1572872 | tf_op jit(solution)/shard_map/ppermute | solution.py:372
  139.8 13.2 %copy-start.11 = (bf16[256,1024]{1,0:T(8,128)(2,1)}, bf16[256,1024]{1,0:T(8,128)(2,1)S(1)}, u32[]{:S(2)}) copy-start(bf16[256,1024]{1,0:T(8,128)(2,1)S(1)} %add_update.6.refs_0_.old_ref) | copy-start | bytes 1572868
  139.8 10.5 %collective-permute-start.17 = (bf16[256,1024]{1,0:T(8,128)(2,1)S(1)}, bf16[256,1024]{1,0:T(8,128)(2,1)S(1)}, u32[]{:S(2)}, u32[]{:S(2)}) collective-permute-start(bf16[256,1024]{1,0:T(8,128)(2,1)S(1)} %add_update.6.refs_0_.old_ref), channel_id=1, source_target_pairs={{0,1},{1,0},{2,3},{3,2},{4,5},{5,4},{6,7},{7,6},{8,9},{9,8},{10,11... | collective-permute-start | bytes 1572872 | tf_op jit(solution)/shard_map/ppermute | solution.py:369
  150.2 2.8 %copy-start.9 = (bf16[256,1024]{1,0:T(8,128)(2,1)}, bf16[256,1024]{1,0:T(8,128)(2,1)S(1)}, u32[]{:S(2)}) copy-start(bf16[256,1024]{1,0:T(8,128)(2,1)S(1)} %add_update.7.refs_0_.old_ref) | copy-start | bytes 1572868
  150.2 2.8 %collective-permute-start.22 = (bf16[256,1024]{1,0:T(8,128)(2,1)S(1)}, bf16[256,1024]{1,0:T(8,128)(2,1)S(1)}, u32[]{:S(2)}, u32[]{:S(2)}) collective-permute-start(bf16[256,1024]{1,0:T(8,128)(2,1)S(1)} %add_update.7.refs_0_.old_ref), channel_id=1, source_target_pairs={{0,1},{1,0},{2,3},{3,2},{4,5},{5,4},{6,7},{7,6},{8,9},{9,8},{10,11... | collective-permute-start | bytes 1572872 | tf_op jit(solution)/shard_map/ppermute | solution.py:369
  155.7 2.8 %copy-start.17 = (bf16[256,512]{1,0:T(8,128)(2,1)}, bf16[256,512]{1,0:T(8,128)(2,1)S(1)}, u32[]{:S(2)}) copy-start(bf16[256,512]{1,0:T(8,128)(2,1)S(1)} %get-tuple-element.56.refs_2_) | copy-start | bytes 786436
  158.5 2.0 collective-permute-start.23
  160.5 2.8 %copy-start = (bf16[3,512,2048]{2,1,0:T(8,128)(2,1)S(1)}, bf16[3,512,2048]{2,1,0:T(8,128)(2,1)}, u32[]{:S(2)}) copy-start(bf16[3,512,2048]{2,1,0:T(8,128)(2,1)} %w_out_ref.11) | copy-start | bytes 18874372
  163.3 4.5 %copy-start.27 = (bf16[2,64,512]{2,1,0:T(8,128)(2,1)S(1)}, bf16[2,64,512]{2,1,0:T(8,128)(2,1)}, u32[]{:S(2)}) copy-start(bf16[2,64,512]{2,1,0:T(8,128)(2,1)} %copy-done.26) | copy-start | bytes 393220
  163.3 5.4 %copy-start.25 = (bf16[2,64,512]{2,1,0:T(8,128)(2,1)S(1)}, bf16[2,64,512]{2,1,0:T(8,128)(2,1)}, u32[]{:S(2)}) copy-start(bf16[2,64,512]{2,1,0:T(8,128)(2,1)} %copy-done.24) | copy-start | bytes 393220
  163.3 10.6 %copy-start.16 = (bf16[256,512]{1,0:T(8,128)(2,1)S(1)}, bf16[256,512]{1,0:T(8,128)(2,1)}, u32[]{:S(2)}) copy-start(bf16[256,512]{1,0:T(8,128)(2,1)} %copy-done.15) | copy-start | bytes 786436
  163.3 10.6 %copy-start.18 = (bf16[256,512]{1,0:T(8,128)(2,1)S(1)}, bf16[256,512]{1,0:T(8,128)(2,1)}, u32[]{:S(2)}) copy-start(bf16[256,512]{1,0:T(8,128)(2,1)} %copy-done.17) | copy-start | bytes 786436
  163.3 10.6 %copy-start.20 = (bf16[256,512]{1,0:T(8,128)(2,1)S(1)}, bf16[256,512]{1,0:T(8,128)(2,1)}, u32[]{:S(2)}) copy-start(bf16[256,512]{1,0:T(8,128)(2,1)} %copy-done.19) | copy-start | bytes 786436
  163.3 10.6 %copy-start.23 = (bf16[256,512]{1,0:T(8,128)(2,1)S(1)}, bf16[256,512]{1,0:T(8,128)(2,1)}, u32[]{:S(2)}) copy-start(bf16[256,512]{1,0:T(8,128)(2,1)} %copy-done.22) | copy-start | bytes 786436
  166.2 10.4 %copy-start.12 = (bf16[256,1024]{1,0:T(8,128)(2,1)S(1)}, bf16[256,1024]{1,0:T(8,128)(2,1)}, u32[]{:S(2)}) copy-start(bf16[256,1024]{1,0:T(8,128)(2,1)} %copy-done.11) | copy-start | bytes 1572868
  166.2 10.4 %collective-permute-start.24 = (bf16[256,512]{1,0:T(8,128)(2,1)S(1)}, bf16[256,512]{1,0:T(8,128)(2,1)S(1)}, u32[]{:S(2)}, u32[]{:S(2)}) collective-permute-start(bf16[256,512]{1,0:T(8,128)(2,1)S(1)} %get-tuple-element.59), channel_id=1, source_target_pairs={{0,2},{1,3},{2,0},{3,1},{4,6},{5,7},{6,4},{7,5},{8,10},{9,11},{10,... | collective-permute-start | bytes 786440 | tf_op jit(solution)/shard_map/ppermute | solution.py:372
  167.8 5.5 %collective-permute-start.25 = (bf16[2,64,512]{2,1,0:T(8,128)(2,1)S(1)}, bf16[2,64,512]{2,1,0:T(8,128)(2,1)S(1)}, u32[]{:S(2)}, u32[]{:S(2)}) collective-permute-start(bf16[2,64,512]{2,1,0:T(8,128)(2,1)S(1)} %copy-done.27), channel_id=1, source_target_pairs={{0,8},{8,16},{16,24},{24,28},{28,20},{20,12},{12,4},{4,0},{1,9},{9... | collective-permute-start | bytes 393224 | tf_op jit(solution)/shard_map/ppermute | solution.py:415
  168.7 5.2 %collective-permute-start.26 = (bf16[2,64,512]{2,1,0:T(8,128)(2,1)S(1)}, bf16[2,64,512]{2,1,0:T(8,128)(2,1)S(1)}, u32[]{:S(2)}, u32[]{:S(2)}) collective-permute-start(bf16[2,64,512]{2,1,0:T(8,128)(2,1)S(1)} %copy-done.25), channel_id=1, source_target_pairs={{8,0},{16,8},{24,16},{28,24},{20,28},{12,20},{4,12},{0,4},{9,1},{1... | collective-permute-start | bytes 393224 | tf_op jit(solution)/shard_map/ppermute | solution.py:414
  176.6 5.3 %collective-permute-start.27 = (bf16[256,512]{1,0:T(8,128)(2,1)}, bf16[256,512]{1,0:T(8,128)(2,1)S(1)}, u32[]{:S(2)}, u32[]{:S(2)}) collective-permute-start(bf16[256,512]{1,0:T(8,128)(2,1)} %attention.11.own_ref), channel_id=1, source_target_pairs={{0,1},{1,0},{2,3},{3,2},{4,5},{5,4},{6,7},{7,6},{8,9},{9,8},{10,11... | collective-permute-start | bytes 786440 | tf_op jit(solution)/shard_map/ppermute | solution.py:369
  177.7 18.6 %all-to-all-start.2 = ((bf16[8,32,512]{2,1,0:T(8,128)(2,1)}), bf16[8,32,512]{2,1,0:T(8,128)(2,1)S(1)}, u32[]{:S(2)}, u32[]{:S(2)}) async-start(bf16[8,32,512]{2,1,0:T(8,128)(2,1)} %finish.2), calls=%async_computation.2 | async-start | bytes 524288 | tf_op jit(solution)/shard_map/all_to_all | solution.py:453
  181.9 2.8 %copy-start.1 = (bf16[3,512,2048]{2,1,0:T(8,128)(2,1)S(1)}, bf16[3,512,2048]{2,1,0:T(8,128)(2,1)}, u32[]{:S(2)}) copy-start(bf16[3,512,2048]{2,1,0:T(8,128)(2,1)} %w_out_ref.11) | copy-start | bytes 18874372
  184.7 11.3 %copy-start.10 = (bf16[256,1024]{1,0:T(8,128)(2,1)S(1)}, bf16[256,1024]{1,0:T(8,128)(2,1)}, u32[]{:S(2)}) copy-start(bf16[256,1024]{1,0:T(8,128)(2,1)} %copy-done.9) | copy-start | bytes 1572868
  187.4 8.5 %collective-permute-start.28 = (bf16[256,512]{1,0:T(8,128)(2,1)S(1)}, bf16[256,512]{1,0:T(8,128)(2,1)S(1)}, u32[]{:S(2)}, u32[]{:S(2)}) collective-permute-start(bf16[256,512]{1,0:T(8,128)(2,1)S(1)} %get-tuple-element.64), channel_id=1, source_target_pairs={{0,2},{1,3},{2,0},{3,1},{4,6},{5,7},{6,4},{7,5},{8,10},{9,11},{10,... | collective-permute-start | bytes 786440 | tf_op jit(solution)/shard_map/ppermute | solution.py:372
  (6 other events, 16.2 us)
